TPU v7x, 32 devices: a whole 2x2x4 slice. The times are simulated.
32 devices in a mesh: sp: 8 (over z, y), tp: 4 (over x, core).
Axes of the slice: x: 2, y: 2, z: 4, core: 2. Of those that a mesh axis runs over, the one named last changes fastest.
Arguments:
- glu_value: bfloat16 [4096, 2048], P('sp', 'tp'), may hold values from -640 to 640
- glu_gate: bfloat16 [4096, 2048], P('sp', 'tp'), may hold values from -9 to 9
- conv_kernel: float32 [31, 2048], P(None, 'tp'), may hold values from -1 to 1
- norm_gain: float32 [2048], P('tp'), may hold values from 0.1 to 1.9
- mix_weight: bfloat16 [2048, 2048], P('tp'), may hold values from -0.125 to 0.125
- residual: bfloat16 [4096, 2048], P(('sp', 'tp')), may hold values from -6 to 6
- resid_gain: float32 [2048], replicated, may hold values from 0.1 to 1.9
- expert_ids: int32 [4096, 2], P(('sp', 'tp')), may hold values from 0 to 7, all different within a row; in each aligned block of 128 rows (0 to 127, 128 to 255, ...) at most 64 rows name the same one
- route_weight: float32 [4096, 2], P(('sp', 'tp')), may hold values from 0.05 to 0.5
- w_gate: bfloat16 [8, 2048, 2048], P('sp', None, 'tp'), may hold values from -0.5 to 0.5
- w_up: bfloat16 [8, 2048, 2048], P('sp', None, 'tp'), may hold values from -0.5 to 0.5
- w_down: bfloat16 [8, 2048, 2048], P('sp', 'tp'), may hold values from -0.03125 to 0.03125
- out_gain: float32 [2048], replicated, may hold values from 0.1 to 1.9
Outputs:
- blended: bfloat16 [4096, 2048], P(('sp', 'tp'))
Inputs may be any that keep to these rules, and one draw needn't show every extreme that they name: `expert_ids`: in each aligned block of 128 rows (the rows of one device) no expert is named by more than 64 rows, a bound that some block reaches.
All inputs are finite; a program needn't handle non-finite values.
Results may differ from a plain program's by a relative error of at most 0.015.
Values may be sent and summed in bfloat16 or wider, within the bound.
No kernel may reach another device: no remote copies, remote signals or barrier semaphores. Data moves between devices by JAX's collectives and lax.ppermute only.
A program may use at most 128 MiB of HBM per device.

v0:
```python
import jax
import jax.numpy as jnp
from jax import lax
from jax.experimental import pallas as pl
from jax.experimental.pallas import tpu as pltpu
from jax.sharding import PartitionSpec as P


EPSILON = 1e-05
LIMIT = 7.0
SLOPE = 1.702


def shifted(block, axis, distance):
    devices = range(lax.axis_size(axis))
    route = [(i - distance, i) for i in devices if i - distance in devices]
    return lax.ppermute(block, axis, route)


def swapped(block, axis, bit):
    return lax.ppermute(block, axis, [(i, i ^ bit) for i in range(lax.axis_size(axis))])


def folded_ring(length):
    return list(range(0, length, 2)) + list(range(1, length, 2))[::-1]


def around(block, distance):
    count = lax.axis_size("sp")
    order = folded_ring(count // 2)
    route = []
    for place, line in enumerate(order):
        target = order[(place + distance) % len(order)]
        route += [(2 * line, 2 * target), (2 * line + 1, 2 * target + 1)]
    return lax.ppermute(block, "sp", route)


def normalize(values, gain_vector):
    centre = jnp.mean(values, axis=-1, keepdims=True)
    spread = jnp.mean(jnp.square(values - centre), axis=-1, keepdims=True)
    return (values - centre) * lax.rsqrt(spread + EPSILON) * gain_vector


def matmul(a, b):
    return jnp.dot(a, b, preferred_element_type=jnp.float32)


def expert_activity(tokens, gate_matrix, up_matrix):
    gated = jnp.minimum(matmul(tokens, gate_matrix), LIMIT)
    upper = jnp.clip(matmul(tokens, up_matrix), -LIMIT, LIMIT)
    return ((upper + 1.0) * gated * jax.nn.sigmoid(SLOPE * gated)).astype(jnp.bfloat16)


def expert_kernel(near, far, gate_matrix, up_matrix, down_matrix, keep, pass_on, send):
    def product(tokens):
        gated = jnp.minimum(matmul(tokens, gate_matrix[...]), LIMIT)
        upper = jnp.clip(matmul(tokens, up_matrix[...]), -LIMIT, LIMIT)
        activity = (upper + 1.0) * gated / (1.0 + jnp.exp(-SLOPE * gated))
        return matmul(activity.astype(jnp.bfloat16), down_matrix[...])

    send[...] = product(far[...]).astype(jnp.bfloat16)
    sums = product(near[...])
    half = keep.shape[0]
    keep[...] = sums[:half]
    pass_on[...] = sums[half:]


def expert_step(near, far, gate_matrix, up_matrix, down_matrix):
    rows, width = near.shape
    vmem = pl.BlockSpec(memory_space=pltpu.VMEM)
    return pl.pallas_call(
        expert_kernel,
        out_shape=(
            jax.ShapeDtypeStruct((rows // 2, width), jnp.float32),
            jax.ShapeDtypeStruct((rows // 2, width), jnp.float32),
            jax.ShapeDtypeStruct((rows, width), jnp.bfloat16),
        ),
        in_specs=[vmem] * 5,
        out_specs=(vmem,) * 3,
        compiler_params=pltpu.CompilerParams(vmem_limit_bytes=40 * 2**20),
        cost_estimate=pl.CostEstimate(
            flops=12 * rows * width * gate_matrix.shape[1], transcendentals=0, bytes_accessed=0
        ),
        name="expert_step",
    )(near, far, gate_matrix, up_matrix, down_matrix)


def gated_rows(value, gate):
    return (value.astype(jnp.float32) * jax.nn.sigmoid(gate.astype(jnp.float32))).astype(jnp.bfloat16)


def convolve(glu_value, glu_gate, conv_kernel, norm_gain):
    reach_back = conv_kernel.shape[0] - 1
    length, channels = glu_value.shape
    tail = slice(length - reach_back, length)
    before_rows = shifted(gated_rows(glu_value[tail], glu_gate[tail]), "sp", 1)
    gated_in = gated_rows(glu_value, glu_gate)
    extended = jnp.concatenate([before_rows, gated_in], axis=0).astype(jnp.float32)
    convolved = jnp.zeros(gated_in.shape, jnp.float32)
    for offset in range(reach_back + 1):
        convolved = convolved + conv_kernel[offset] * extended[offset : offset + length]
    channel_sum, squares = lax.psum(
        (jnp.sum(convolved, axis=1), jnp.sum(convolved * convolved, axis=1)), "tp"
    )
    channels = channels * lax.axis_size("tp")
    centre = channel_sum / channels
    spread = squares / channels - centre * centre
    normed = (convolved - centre[:, None]) * lax.rsqrt(spread[:, None] + EPSILON) * norm_gain
    return jax.nn.silu(normed).astype(jnp.bfloat16)


def scattered_product(mix_in, mix_weight):
    count = lax.axis_size("tp")
    rows = mix_in.shape[0] // count
    here = lax.axis_index("tp")

    def product(d):
        own = lax.dynamic_slice_in_dim(mix_in, (here ^ d) * rows, rows, axis=0)
        return matmul(own, mix_weight)

    parts = [None] * count
    for d in reversed(range(count)):
        parts[d] = product(d)
    bit = 1
    while bit < count:
        kept = {}
        for d in reversed(range(0, count, 2 * bit)):
            arrived = swapped(parts[d + bit].astype(jnp.bfloat16), "tp", bit)
            kept[d] = parts[d] + arrived.astype(jnp.float32)
        parts = [kept.get(d) for d in range(count)]
        bit *= 2
    return parts[0]


def slots_of(ids, weights, expert, capacity):
    named = (ids == expert).astype(jnp.float32)
    chosen = jnp.sum(named, axis=1)
    count = ids.shape[0]
    earlier = (
        lax.broadcasted_iota(jnp.int32, (count, count), 0)
        > lax.broadcasted_iota(jnp.int32, (count, count), 1)
    ).astype(jnp.float32)
    rank = jnp.sum(earlier * chosen[None, :], axis=1)
    places = lax.broadcasted_iota(jnp.int32, (count, capacity), 1).astype(jnp.float32)
    onehot = ((places == rank[:, None]) & (chosen[:, None] > 0)).astype(jnp.bfloat16)
    return onehot, jnp.sum(named * weights, axis=1)


def routed_ring(hidden, ids, weights, gate_local, up_local, down_local, capacity):
    steps = lax.axis_size("sp") // 2
    here = lax.axis_index("sp").astype(jnp.float32)
    other = (lax.axis_index("sp") ^ 1).astype(jnp.float32)
    top = ids.shape[1]
    table = jnp.concatenate([ids.astype(jnp.float32), weights], axis=1)
    tables = [table]
    for s in range(1, steps):
        tables.append(around(table, s))
    block = hidden
    carried = None
    for s in range(steps):
        if s + 1 < steps:
            following = around(block, 1)
        own_hot, own_weight = slots_of(tables[s][:, :top], tables[s][:, top:], here, capacity)
        far_hot, far_weight = slots_of(tables[s][:, :top], tables[s][:, top:], other, capacity)
        far_rows = matmul(far_hot.T, block).astype(jnp.bfloat16)
        arrived = swapped(far_rows, "sp", 1)
        picked = matmul(own_hot.T, block).astype(jnp.bfloat16)
        own_x = swapped(picked, "tp", 2)
        far_x = swapped(arrived, "tp", 2)
        near = jnp.concatenate([picked, arrived, own_x, far_x], axis=0)
        far = swapped(near, "tp", 1)
        keep, pass_on, send = expert_step(near, far, gate_local, up_local, down_local)
        from_core = swapped(send, "tp", 1)
        half = keep.shape[0]
        pass_on = (pass_on + from_core[half:].astype(jnp.float32)).astype(jnp.bfloat16)
        from_chip = swapped(pass_on, "tp", 2)
        sums = keep + from_core[:half].astype(jnp.float32) + from_chip.astype(jnp.float32)
        sums = sums.astype(jnp.bfloat16)
        mine, theirs = sums[:capacity], sums[capacity:]
        theirs = swapped(theirs, "sp", 1)
        share = own_weight[:, None] * matmul(own_hot, mine) + far_weight[:, None] * matmul(far_hot, theirs)
        if s == 0:
            own_share = share
        else:
            share = (share if carried is None else carried.astype(jnp.float32) + share).astype(jnp.bfloat16)
        if s:
            carried = around(share, 1)
        block = following
    return own_share + carried.astype(jnp.float32)


def slot_layout(route_ids, experts, capacity):
    row_count, top_count = route_ids.shape
    flat_ids = route_ids.reshape(row_count * top_count)
    onehot = (flat_ids[:, None] == jnp.arange(experts, dtype=jnp.int32)[None, :]).astype(jnp.int32)
    before = jnp.cumsum(onehot, axis=0) - onehot
    slot_rank = jnp.sum(before * onehot, axis=1)
    position = flat_ids * capacity + slot_rank
    owners = jnp.arange(row_count * top_count, dtype=jnp.int32) // top_count
    slot_table = jnp.full((experts * capacity,), row_count, jnp.int32).at[position].set(owners)
    return (slot_table, position.reshape(row_count, top_count))


def routed_exchange(hidden, ids, weights, gate_local, up_local, down_local, capacity):
    experts = lax.axis_size("sp")
    own_count, width = hidden.shape
    top_count = ids.shape[1]
    own_table, positions = slot_layout(ids, experts, capacity)
    padded = jnp.concatenate([hidden, jnp.zeros((1, width), jnp.bfloat16)], axis=0)
    dispatched = padded[own_table].reshape(experts, capacity, width)
    arrived = lax.all_to_all(dispatched, "sp", split_axis=0, concat_axis=0, tiled=True)
    gathered = lax.all_gather(arrived[None], "tp", axis=0, tiled=True)
    activity = expert_activity(gathered.reshape(-1, width), gate_local, up_local)
    expert_out = lax.psum_scatter(
        matmul(activity, down_local).astype(jnp.bfloat16), "tp", scatter_dimension=0, tiled=True
    )
    expert_out = expert_out.reshape(experts, capacity, width)
    returned = lax.all_to_all(expert_out, "sp", split_axis=0, concat_axis=0, tiled=True)
    picked = returned.reshape(experts * capacity, width)[positions.reshape(-1)]
    picked = picked.reshape(own_count, top_count, width)
    return jnp.einsum("tk,tkd->td", weights, picked.astype(jnp.float32))


def shards(
    glu_value,
    glu_gate,
    conv_kernel,
    norm_gain,
    mix_weight,
    residual,
    resid_gain,
    expert_ids,
    route_weight,
    w_gate,
    w_up,
    w_down,
    out_gain,
):
    mix_in = convolve(glu_value, glu_gate, conv_kernel, norm_gain)
    mix_in, expert_ids, route_weight = lax.optimization_barrier((mix_in, expert_ids, route_weight))
    mixed_rows = scattered_product(mix_in, mix_weight)
    hidden = normalize(residual.astype(jnp.float32) + mixed_rows, resid_gain).astype(jnp.bfloat16)
    experts = lax.axis_size("sp")
    own_count, top_count = expert_ids.shape
    capacity = 2 * own_count * top_count // experts
    whole_rows = (experts // 2 - 1) * own_count + experts // 2 * capacity
    padded_rows = (experts - 1) * capacity
    ring = lax.axis_size("tp") == 4 and whole_rows <= 2 * padded_rows
    route = routed_ring if ring else routed_exchange
    routed_sum = route(hidden, expert_ids, route_weight, w_gate[0], w_up[0], w_down[0], capacity)
    return normalize(hidden.astype(jnp.float32) + routed_sum, out_gain).astype(jnp.bfloat16)


def solution(mesh):
    in_specs = (
        P("sp", "tp"),
        P("sp", "tp"),
        P(None, "tp"),
        P("tp"),
        P("tp", None),
        P(("sp", "tp"), None),
        P(),
        P(("sp", "tp"), None),
        P(("sp", "tp"), None),
        P("sp", None, "tp"),
        P("sp", None, "tp"),
        P("sp", "tp", None),
        P(),
    )
    out_specs = P(("sp", "tp"), None)
    return jax.shard_map(shards, mesh=mesh, in_specs=in_specs, out_specs=out_specs, check_vma=False)
```

profile of v0, /device:TPU:0, one launch (start us, length us, event | category | flops | bytes accessed | tf_op | source)
XLA Modules:
  0.0 178.1 jit_solution(11371248357588406857)
XLA Ops:
  1.0 4.9 %collective-permute-start = (bf16[30,512]{1,0:T(8,128)(2,1)S(1)}, bf16[30,512]{1,0:T(8,128)(2,1)S(1)}, u32[]{:S(2)}, u32[]{:S(2)}) collective-permute-start(bf16[30,512]{1,0:T(8,128)(2,1)S(1)} %multiply_convert_fusion.4), channel_id=1, source_target_pairs={{0,4},{4,8},{8,12},{12,16},{16,20},{20,24},{24,28},{1,5},{5,9},{9,... | collective-permute-start | bytes 92168 | tf_op jit(solution)/shard_map/ppermute | solution.py:17
  9.8 5.1 %fusion.103 = (f32[512]{0:T(512)S(1)}, f32[512]{0:T(512)S(1)}, f32[512,512]{1,0:T(8,128)S(1)}) fusion(f32[542,512]{1,0:T(8,128)S(1)} %maximum_convert_fusion, f32[512]{0:T(512)S(1)} %bitcast.91, f32[512]{0:T(512)S(1)} %bitcast.92, f32[512]{0:T(512)S(1)} %bitcast.63, f32[512]{0:T(512)S(1)} %bitcast.64, f32[512]{0:T(512)S(1)} %bitcast.65, ...), kind=kLoop, calls=%fused_computation.227 | loop fusion | flops 16776192 | bytes 33622016 | tf_op jit(solution)/shard_map/reduce_sum | solution.py:103
  14.9 6.3 %all-reduce = (f32[512]{0:T(512)S(1)}, f32[512]{0:T(512)S(1)}) all-reduce(f32[512]{0:T(512)S(1)} %get-tuple-element.36, f32[512]{0:T(512)S(1)} %get-tuple-element.35), channel_id=1, replica_groups=mesh['sp'=8,'tp'=4] {'tp'}, use_global_device_ids=true, to_apply=%region_3.0 | all-reduce | flops 1024 | bytes 8192 | tf_op jit(solution)/shard_map/psum | solution.py:102
  21.9 2.6 %collective-permute-start.11 = (f32[128,4]{0,1:T(4,128)S(1)}, f32[128,4]{0,1:T(4,128)S(1)}, u32[]{:S(2)}, u32[]{:S(2)}) collective-permute-start(f32[128,4]{0,1:T(4,128)S(1)} %pad_maximum_fusion.4), channel_id=1, source_target_pairs={{0,16},{4,20},{16,24},{20,28},{24,8},{28,12},{8,0},{12,4},{1,17},{... | collective-permute-start | bytes 6152 | tf_op jit(solution)/shard_map/ppermute | solution.py:35
  31.9 11.7 %collective-permute-done.3 = bf16[128,2048]{1,0:T(8,128)(2,1)S(1)} collective-permute-done((bf16[128,2048]{1,0:T(8,128)(2,1)S(1)}, bf16[128,2048]{1,0:T(8,128)(2,1)S(1)}, u32[]{:S(2)}, u32[]{:S(2)}) %collective-permute-start.3) | collective-permute-done | bytes 524320 | tf_op jit(solution)/shard_map/ppermute | solution.py:21
  46.7 11.4 %collective-permute-done.12 = bf16[128,2048]{1,0:T(8,128)(2,1)S(1)} collective-permute-done((bf16[128,2048]{1,0:T(8,128)(2,1)S(1)}, bf16[128,2048]{1,0:T(8,128)(2,1)S(1)}, u32[]{:S(2)}, u32[]{:S(2)}) %collective-permute-start.12) | collective-permute-done | bytes 524320 | tf_op jit(solution)/shard_map/ppermute | solution.py:35
  60.1 2.5 %collective-permute-start.22 = (bf16[128,2048]{1,0:T(8,128)(2,1)S(1)}, bf16[128,2048]{1,0:T(8,128)(2,1)S(1)}, u32[]{:S(2)}, u32[]{:S(2)}) collective-permute-start(bf16[128,2048]{1,0:T(8,128)(2,1)S(1)} %collective-permute-done.12), channel_id=1, source_target_pairs={{0,16},{4,20},{16,24},{20,28},{24,8},{28,12},{8,0},{12,4},{1,17},{... | collective-permute-start | bytes 1572872 | tf_op jit(solution)/shard_map/ppermute | solution.py:35
  68.5 4.5 %collective-permute-done.22 = bf16[128,2048]{1,0:T(8,128)(2,1)S(1)} collective-permute-done((bf16[128,2048]{1,0:T(8,128)(2,1)S(1)}, bf16[128,2048]{1,0:T(8,128)(2,1)S(1)}, u32[]{:S(2)}, u32[]{:S(2)}) %collective-permute-start.22) | collective-permute-done | bytes 524320 | tf_op jit(solution)/shard_map/ppermute | solution.py:35
  82.3 2.3 %collective-permute-done.24 = bf16[64,2048]{1,0:T(8,128)(2,1)S(1)} collective-permute-done((bf16[64,2048]{1,0:T(8,128)(2,1)S(1)}, bf16[64,2048]{1,0:T(8,128)(2,1)S(1)}, u32[]{:S(2)}, u32[]{:S(2)}) %collective-permute-start.24) | collective-permute-done | bytes 262176 | tf_op jit(solution)/shard_map/ppermute | solution.py:21
  85.7 4.5 %collective-permute-done.25 = bf16[64,2048]{1,0:T(8,128)(2,1)S(1)} collective-permute-done((bf16[64,2048]{1,0:T(8,128)(2,1)S(1)}, bf16[64,2048]{1,0:T(8,128)(2,1)S(1)}, u32[]{:S(2)}, u32[]{:S(2)}) %collective-permute-start.25) | collective-permute-done | bytes 262176 | tf_op jit(solution)/shard_map/ppermute | solution.py:21
  92.5 3.6 %expert_step.5 = (f32[128,2048]{1,0:T(8,128)S(1)}, f32[128,2048]{1,0:T(8,128)S(1)}, bf16[256,2048]{1,0:T(8,128)(2,1)S(1)}) custom-call(bf16[256,2048]{1,0:T(8,128)(2,1)S(1)} %pad_maximum_fusion.1.near, bf16[256,2048]{1,0:T(8,128)(2,1)S(1)} %collective-permute-done.16.far, bf16[2048,512]{1,0:T(8,128)(2,1)S(1)} %bitcast.50, bf16[2048,512]{1,0:T(8,128)(2,1)S(1)} %bitcast.54, ...), custom_call_target="tpu_custom_call" | custom-call | flops 3221225472 | tf_op jit(solution)/shard_map/expert_step/pallas_call | solution.py:71
  101.6 5.4 %collective-permute-done.34 = bf16[64,2048]{1,0:T(8,128)(2,1)S(1)} collective-permute-done((bf16[64,2048]{1,0:T(8,128)(2,1)S(1)}, bf16[64,2048]{1,0:T(8,128)(2,1)S(1)}, u32[]{:S(2)}, u32[]{:S(2)}) %collective-permute-start.34) | collective-permute-done | bytes 262176 | tf_op jit(solution)/shard_map/ppermute | solution.py:21
  107.1 5.1 %collective-permute-done.35 = bf16[64,2048]{1,0:T(8,128)(2,1)S(1)} collective-permute-done((bf16[64,2048]{1,0:T(8,128)(2,1)S(1)}, bf16[64,2048]{1,0:T(8,128)(2,1)S(1)}, u32[]{:S(2)}, u32[]{:S(2)}) %collective-permute-start.35) | collective-permute-done | bytes 262176 | tf_op jit(solution)/shard_map/ppermute | solution.py:21
  112.4 3.6 %expert_step.6 = (f32[128,2048]{1,0:T(8,128)S(1)}, f32[128,2048]{1,0:T(8,128)S(1)}, bf16[256,2048]{1,0:T(8,128)(2,1)S(1)}) custom-call(bf16[256,2048]{1,0:T(8,128)(2,1)S(1)} %pad_maximum_fusion.2.near, bf16[256,2048]{1,0:T(8,128)(2,1)S(1)} %collective-permute-done.26.far, bf16[2048,512]{1,0:T(8,128)(2,1)S(1)} %bitcast.51, bf16[2048,512]{1,0:T(8,128)(2,1)S(1)} %bitcast.55, ...), custom_call_target="tpu_custom_call" | custom-call | flops 3221225472 | tf_op jit(solution)/shard_map/expert_step/pallas_call | solution.py:71
  117.9 3.6 %expert_step.4 = (f32[128,2048]{1,0:T(8,128)S(1)}, f32[128,2048]{1,0:T(8,128)S(1)}, bf16[256,2048]{1,0:T(8,128)(2,1)S(1)}) custom-call(bf16[256,2048]{1,0:T(8,128)(2,1)S(1)} %pad_maximum_fusion.near, bf16[256,2048]{1,0:T(8,128)(2,1)S(1)} %collective-permute-done.7.far, bf16[2048,512]{1,0:T(8,128)(2,1)S(1)} %bitcast.52, bf16[2048,512]{1,0:T(8,128)(2,1)S(1)} %bitcast.56, ...), custom_call_target="tpu_custom_call" | custom-call | flops 3221225472 | tf_op jit(solution)/shard_map/expert_step/pallas_call | solution.py:71
  121.6 3.9 %expert_step.7 = (f32[128,2048]{1,0:T(8,128)S(1)}, f32[128,2048]{1,0:T(8,128)S(1)}, bf16[256,2048]{1,0:T(8,128)(2,1)S(1)}) custom-call(bf16[256,2048]{1,0:T(8,128)(2,1)S(1)} %pad_maximum_fusion.3.near, bf16[256,2048]{1,0:T(8,128)(2,1)S(1)} %collective-permute-done.36.far, bf16[2048,512]{1,0:T(8,128)(2,1)S(1)} %bitcast.53, bf16[2048,512]{1,0:T(8,128)(2,1)S(1)} %bitcast.57, ...), custom_call_target="tpu_custom_call" | custom-call | flops 3221225472 | tf_op jit(solution)/shard_map/expert_step/pallas_call | solution.py:71
  126.0 4.6 %collective-permute-done.18 = bf16[128,2048]{1,0:T(8,128)(2,1)S(1)} collective-permute-done((bf16[128,2048]{1,0:T(8,128)(2,1)S(1)}, bf16[128,2048]{1,0:T(8,128)(2,1)S(1)}, u32[]{:S(2)}, u32[]{:S(2)}) %collective-permute-start.18) | collective-permute-done | bytes 524320 | tf_op jit(solution)/shard_map/ppermute | solution.py:21
  133.4 4.9 %collective-permute-done.19 = bf16[64,2048]{1,0:T(8,128)(2,1)S(1)} collective-permute-done((bf16[64,2048]{1,0:T(8,128)(2,1)S(1)}, bf16[64,2048]{1,0:T(8,128)(2,1)S(1)}, u32[]{:S(2)}, u32[]{:S(2)}) %collective-permute-start.19) | collective-permute-done | bytes 262176 | tf_op jit(solution)/shard_map/ppermute | solution.py:21
  140.3 4.4 %collective-permute-done.28 = bf16[128,2048]{1,0:T(8,128)(2,1)S(1)} collective-permute-done((bf16[128,2048]{1,0:T(8,128)(2,1)S(1)}, bf16[128,2048]{1,0:T(8,128)(2,1)S(1)}, u32[]{:S(2)}, u32[]{:S(2)}) %collective-permute-start.28) | collective-permute-done | bytes 524320 | tf_op jit(solution)/shard_map/ppermute | solution.py:21
  147.7 3.1 %collective-permute-done.20 = bf16[128,2048]{1,0:T(8,128)(2,1)S(1)} collective-permute-done((bf16[128,2048]{1,0:T(8,128)(2,1)S(1)}, bf16[128,2048]{1,0:T(8,128)(2,1)S(1)}, u32[]{:S(2)}, u32[]{:S(2)}) %collective-permute-start.20) | collective-permute-done | bytes 524320 | tf_op jit(solution)/shard_map/ppermute | solution.py:35
  154.0 3.9 %collective-permute-done.38 = bf16[128,2048]{1,0:T(8,128)(2,1)S(1)} collective-permute-done((bf16[128,2048]{1,0:T(8,128)(2,1)S(1)}, bf16[128,2048]{1,0:T(8,128)(2,1)S(1)}, u32[]{:S(2)}, u32[]{:S(2)}) %collective-permute-start.38) | collective-permute-done | bytes 524320 | tf_op jit(solution)/shard_map/ppermute | solution.py:21
  160.6 2.8 %collective-permute-done.30 = bf16[128,2048]{1,0:T(8,128)(2,1)S(1)} collective-permute-done((bf16[128,2048]{1,0:T(8,128)(2,1)S(1)}, bf16[128,2048]{1,0:T(8,128)(2,1)S(1)}, u32[]{:S(2)}, u32[]{:S(2)}) %collective-permute-start.30) | collective-permute-done | bytes 524320 | tf_op jit(solution)/shard_map/ppermute | solution.py:35
  166.6 3.0 %collective-permute-done.9 = bf16[128,2048]{1,0:T(8,128)(2,1)S(1)} collective-permute-done((bf16[128,2048]{1,0:T(8,128)(2,1)S(1)}, bf16[128,2048]{1,0:T(8,128)(2,1)S(1)}, u32[]{:S(2)}, u32[]{:S(2)}) %collective-permute-start.9) | collective-permute-done | bytes 524320 | tf_op jit(solution)/shard_map/ppermute | solution.py:21
  171.5 4.8 %collective-permute-done.10 = bf16[64,2048]{1,0:T(8,128)(2,1)S(1)} collective-permute-done((bf16[64,2048]{1,0:T(8,128)(2,1)S(1)}, bf16[64,2048]{1,0:T(8,128)(2,1)S(1)}, u32[]{:S(2)}, u32[]{:S(2)}) %collective-permute-start.10) | collective-permute-done | bytes 262176 | tf_op jit(solution)/shard_map/ppermute | solution.py:21
  (161 shorter events, 64.7 us)
Async XLA Ops:
  25.9 20.8 %collective-permute-start.31 = (f32[128,4]{0,1:T(4,128)S(1)}, f32[128,4]{0,1:T(4,128)S(1)}, u32[]{:S(2)}, u32[]{:S(2)}) collective-permute-start(f32[128,4]{0,1:T(4,128)S(1)} %pad_maximum_fusion.4), channel_id=1, source_target_pairs={{0,8},{4,12},{16,0},{20,4},{24,16},{28,20},{8,24},{12,28},{1,9},{5... | collective-permute-start | bytes 6152 | tf_op jit(solution)/shard_map/ppermute | solution.py:35
  30.5 13.1 %collective-permute-start.3 = (bf16[128,2048]{1,0:T(8,128)(2,1)S(1)}, bf16[128,2048]{1,0:T(8,128)(2,1)S(1)}, u32[]{:S(2)}, u32[]{:S(2)}) collective-permute-start(bf16[128,2048]{1,0:T(8,128)(2,1)S(1)} %add_convert_fusion.11), channel_id=1, source_target_pairs={{0,2},{1,3},{2,0},{3,1},{4,6},{5,7},{6,4},{7,5},{8,10},{9,11},{10,... | collective-permute-start | bytes 1572872 | tf_op jit(solution)/shard_map/ppermute | solution.py:21
  44.5 13.6 %collective-permute-start.12 = (bf16[128,2048]{1,0:T(8,128)(2,1)S(1)}, bf16[128,2048]{1,0:T(8,128)(2,1)S(1)}, u32[]{:S(2)}, u32[]{:S(2)}) collective-permute-start(bf16[128,2048]{1,0:T(8,128)(2,1)S(1)} %multiply_convert_fusion.1), channel_id=1, source_target_pairs={{0,16},{4,20},{16,24},{20,28},{24,8},{28,12},{8,0},{12,4},{1,17},{... | collective-permute-start | bytes 1572872 | tf_op jit(solution)/shard_map/ppermute | solution.py:35
  60.1 12.8 %collective-permute-start.22 = (bf16[128,2048]{1,0:T(8,128)(2,1)S(1)}, bf16[128,2048]{1,0:T(8,128)(2,1)S(1)}, u32[]{:S(2)}, u32[]{:S(2)}) collective-permute-start(bf16[128,2048]{1,0:T(8,128)(2,1)S(1)} %collective-permute-done.12), channel_id=1, source_target_pairs={{0,16},{4,20},{16,24},{20,28},{24,8},{28,12},{8,0},{12,4},{1,17},{... | collective-permute-start | bytes 1572872 | tf_op jit(solution)/shard_map/ppermute | solution.py:35
  63.1 10.8 %collective-permute-start.14 = (bf16[64,2048]{1,0:T(8,128)(2,1)S(1)}, bf16[64,2048]{1,0:T(8,128)(2,1)S(1)}, u32[]{:S(2)}, u32[]{:S(2)}) collective-permute-start(bf16[64,2048]{1,0:T(8,128)(2,1)S(1)} %convolution_convert_fusion.7), channel_id=1, source_target_pairs={{0,2},{1,3},{2,0},{3,1},{4,6},{5,7},{6,4},{7,5},{8,10},{9,11},{10,... | collective-permute-start | bytes 786440 | tf_op jit(solution)/shard_map/ppermute | solution.py:21
  66.9 14.4 %collective-permute-start.4 = (bf16[64,2048]{1,0:T(8,128)(2,1)S(1)}, bf16[64,2048]{1,0:T(8,128)(2,1)S(1)}, u32[]{:S(2)}, u32[]{:S(2)}) collective-permute-start(bf16[64,2048]{1,0:T(8,128)(2,1)S(1)} %convolution_convert_fusion.8), channel_id=1, source_target_pairs={{0,4},{4,0},{8,12},{12,8},{16,20},{20,16},{24,28},{28,24},{1,5},{5... | collective-permute-start | bytes 786440 | tf_op jit(solution)/shard_map/ppermute | solution.py:21
  74.9 17.5 %collective-permute-start.16 = (bf16[256,2048]{1,0:T(8,128)(2,1)S(1)}, bf16[256,2048]{1,0:T(8,128)(2,1)S(1)}, u32[]{:S(2)}, u32[]{:S(2)}) collective-permute-start(bf16[256,2048]{1,0:T(8,128)(2,1)S(1)} %pad_maximum_fusion.1.near), channel_id=1, source_target_pairs={{0,1},{1,0},{2,3},{3,2},{4,5},{5,4},{6,7},{7,6},{8,9},{9,8},{10,11... | collective-permute-start | bytes 3145736 | tf_op jit(solution)/shard_map/ppermute | solution.py:21
  76.5 14.0 %collective-permute-start.32 = (bf16[128,2048]{1,0:T(8,128)(2,1)S(1)}, bf16[128,2048]{1,0:T(8,128)(2,1)S(1)}, u32[]{:S(2)}, u32[]{:S(2)}) collective-permute-start(bf16[128,2048]{1,0:T(8,128)(2,1)S(1)} %collective-permute-done.22), channel_id=1, source_target_pairs={{0,16},{4,20},{16,24},{20,28},{24,8},{28,12},{8,0},{12,4},{1,17},{... | collective-permute-start | bytes 1572872 | tf_op jit(solution)/shard_map/ppermute | solution.py:35
  81.3 15.2 %collective-permute-start.5 = (bf16[64,2048]{1,0:T(8,128)(2,1)S(1)}, bf16[64,2048]{1,0:T(8,128)(2,1)S(1)}, u32[]{:S(2)}, u32[]{:S(2)}) collective-permute-start(bf16[64,2048]{1,0:T(8,128)(2,1)S(1)} %convolution_convert_fusion.9), channel_id=1, source_target_pairs={{0,2},{1,3},{2,0},{3,1},{4,6},{5,7},{6,4},{7,5},{8,10},{9,11},{10,... | collective-permute-start | bytes 786440 | tf_op jit(solution)/shard_map/ppermute | solution.py:21
  84.6 16.9 %collective-permute-start.6 = (bf16[64,2048]{1,0:T(8,128)(2,1)S(1)}, bf16[64,2048]{1,0:T(8,128)(2,1)S(1)}, u32[]{:S(2)}, u32[]{:S(2)}) collective-permute-start(bf16[64,2048]{1,0:T(8,128)(2,1)S(1)} %collective-permute-done.4), channel_id=1, source_target_pairs={{0,2},{1,3},{2,0},{3,1},{4,6},{5,7},{6,4},{7,5},{8,10},{9,11},{10,... | collective-permute-start | bytes 786440 | tf_op jit(solution)/shard_map/ppermute | solution.py:21
  90.3 22.1 %collective-permute-start.26 = (bf16[256,2048]{1,0:T(8,128)(2,1)S(1)}, bf16[256,2048]{1,0:T(8,128)(2,1)S(1)}, u32[]{:S(2)}, u32[]{:S(2)}) collective-permute-start(bf16[256,2048]{1,0:T(8,128)(2,1)S(1)} %pad_maximum_fusion.2.near), channel_id=1, source_target_pairs={{0,1},{1,0},{2,3},{3,2},{4,5},{5,4},{6,7},{7,6},{8,9},{9,8},{10,11... | collective-permute-start | bytes 3145736 | tf_op jit(solution)/shard_map/ppermute | solution.py:21
  96.1 20.5 %collective-permute-start.17 = (bf16[256,2048]{1,0:T(8,128)(2,1)S(1)}, bf16[256,2048]{1,0:T(8,128)(2,1)S(1)}, u32[]{:S(2)}, u32[]{:S(2)}) collective-permute-start(bf16[256,2048]{1,0:T(8,128)(2,1)S(1)} %get-tuple-element.27), channel_id=1, source_target_pairs={{0,1},{1,0},{2,3},{3,2},{4,5},{5,4},{6,7},{7,6},{8,9},{9,8},{10,11... | collective-permute-start | bytes 3145736 | tf_op jit(solution)/shard_map/ppermute | solution.py:21
  96.5 10.5 %collective-permute-start.34 = (bf16[64,2048]{1,0:T(8,128)(2,1)S(1)}, bf16[64,2048]{1,0:T(8,128)(2,1)S(1)}, u32[]{:S(2)}, u32[]{:S(2)}) collective-permute-start(bf16[64,2048]{1,0:T(8,128)(2,1)S(1)} %convolution_convert_fusion.3), channel_id=1, source_target_pairs={{0,2},{1,3},{2,0},{3,1},{4,6},{5,7},{6,4},{7,5},{8,10},{9,11},{10,... | collective-permute-start | bytes 786440 | tf_op jit(solution)/shard_map/ppermute | solution.py:21
  99.5 12.7 %collective-permute-start.35 = (bf16[64,2048]{1,0:T(8,128)(2,1)S(1)}, bf16[64,2048]{1,0:T(8,128)(2,1)S(1)}, u32[]{:S(2)}, u32[]{:S(2)}) collective-permute-start(bf16[64,2048]{1,0:T(8,128)(2,1)S(1)} %collective-permute-done.33), channel_id=1, source_target_pairs={{0,2},{1,3},{2,0},{3,1},{4,6},{5,7},{6,4},{7,5},{8,10},{9,11},{10,... | collective-permute-start | bytes 786440 | tf_op jit(solution)/shard_map/ppermute | solution.py:21
  101.6 16.3 %collective-permute-start.7 = (bf16[256,2048]{1,0:T(8,128)(2,1)S(1)}, bf16[256,2048]{1,0:T(8,128)(2,1)S(1)}, u32[]{:S(2)}, u32[]{:S(2)}) collective-permute-start(bf16[256,2048]{1,0:T(8,128)(2,1)S(1)} %pad_maximum_fusion.near), channel_id=1, source_target_pairs={{0,1},{1,0},{2,3},{3,2},{4,5},{5,4},{6,7},{7,6},{8,9},{9,8},{10,11... | collective-permute-start | bytes 3145736 | tf_op jit(solution)/shard_map/ppermute | solution.py:21
  116.0 15.7 %collective-permute-start.27 = (bf16[256,2048]{1,0:T(8,128)(2,1)S(1)}, bf16[256,2048]{1,0:T(8,128)(2,1)S(1)}, u32[]{:S(2)}, u32[]{:S(2)}) collective-permute-start(bf16[256,2048]{1,0:T(8,128)(2,1)S(1)} %get-tuple-element.30), channel_id=1, source_target_pairs={{0,1},{1,0},{2,3},{3,2},{4,5},{5,4},{6,7},{7,6},{8,9},{9,8},{10,11... | collective-permute-start | bytes 3145736 | tf_op jit(solution)/shard_map/ppermute | solution.py:21
  116.7 13.9 %collective-permute-start.18 = (bf16[128,2048]{1,0:T(8,128)(2,1)S(1)}, bf16[128,2048]{1,0:T(8,128)(2,1)S(1)}, u32[]{:S(2)}, u32[]{:S(2)}) collective-permute-start(bf16[128,2048]{1,0:T(8,128)(2,1)S(1)} %add_convert_fusion.8), channel_id=1, source_target_pairs={{0,2},{1,3},{2,0},{3,1},{4,6},{5,7},{6,4},{7,5},{8,10},{9,11},{10,... | collective-permute-start | bytes 1572872 | tf_op jit(solution)/shard_map/ppermute | solution.py:21
  121.5 37.5 %collective-permute-start.8 = (bf16[256,2048]{1,0:T(8,128)(2,1)S(1)}, bf16[256,2048]{1,0:T(8,128)(2,1)S(1)}, u32[]{:S(2)}, u32[]{:S(2)}) collective-permute-start(bf16[256,2048]{1,0:T(8,128)(2,1)S(1)} %get-tuple-element.24), channel_id=1, source_target_pairs={{0,1},{1,0},{2,3},{3,2},{4,5},{5,4},{6,7},{7,6},{8,9},{9,8},{10,11... | collective-permute-start | bytes 3145736 | tf_op jit(solution)/shard_map/ppermute | solution.py:21
  125.4 20.7 %collective-permute-start.37 = (bf16[256,2048]{1,0:T(8,128)(2,1)S(1)}, bf16[256,2048]{1,0:T(8,128)(2,1)S(1)}, u32[]{:S(2)}, u32[]{:S(2)}) collective-permute-start(bf16[256,2048]{1,0:T(8,128)(2,1)S(1)} %get-tuple-element.33), channel_id=1, source_target_pairs={{0,1},{1,0},{2,3},{3,2},{4,5},{5,4},{6,7},{7,6},{8,9},{9,8},{10,11... | collective-permute-start | bytes 3145736 | tf_op jit(solution)/shard_map/ppermute | solution.py:21
  131.9 12.8 %collective-permute-start.28 = (bf16[128,2048]{1,0:T(8,128)(2,1)S(1)}, bf16[128,2048]{1,0:T(8,128)(2,1)S(1)}, u32[]{:S(2)}, u32[]{:S(2)}) collective-permute-start(bf16[128,2048]{1,0:T(8,128)(2,1)S(1)} %add_convert_fusion.5), channel_id=1, source_target_pairs={{0,2},{1,3},{2,0},{3,1},{4,6},{5,7},{6,4},{7,5},{8,10},{9,11},{10,... | collective-permute-start | bytes 1572872 | tf_op jit(solution)/shard_map/ppermute | solution.py:21
  138.6 12.2 %collective-permute-start.20 = (bf16[128,2048]{1,0:T(8,128)(2,1)S(1)}, bf16[128,2048]{1,0:T(8,128)(2,1)S(1)}, u32[]{:S(2)}, u32[]{:S(2)}) collective-permute-start(bf16[128,2048]{1,0:T(8,128)(2,1)S(1)} %add_convert_fusion.6), channel_id=1, source_target_pairs={{0,16},{4,20},{16,24},{20,28},{24,8},{28,12},{8,0},{12,4},{1,17},{... | collective-permute-start | bytes 1572872 | tf_op jit(solution)/shard_map/ppermute | solution.py:35
  146.2 11.6 %collective-permute-start.38 = (bf16[128,2048]{1,0:T(8,128)(2,1)S(1)}, bf16[128,2048]{1,0:T(8,128)(2,1)S(1)}, u32[]{:S(2)}, u32[]{:S(2)}) collective-permute-start(bf16[128,2048]{1,0:T(8,128)(2,1)S(1)} %add_convert_fusion.2), channel_id=1, source_target_pairs={{0,2},{1,3},{2,0},{3,1},{4,6},{5,7},{6,4},{7,5},{8,10},{9,11},{10,... | collective-permute-start | bytes 1572872 | tf_op jit(solution)/shard_map/ppermute | solution.py:21
  151.7 11.7 %collective-permute-start.30 = (bf16[128,2048]{1,0:T(8,128)(2,1)S(1)}, bf16[128,2048]{1,0:T(8,128)(2,1)S(1)}, u32[]{:S(2)}, u32[]{:S(2)}) collective-permute-start(bf16[128,2048]{1,0:T(8,128)(2,1)S(1)} %add_convert_fusion.3), channel_id=1, source_target_pairs={{0,16},{4,20},{16,24},{20,28},{24,8},{28,12},{8,0},{12,4},{1,17},{... | collective-permute-start | bytes 1572872 | tf_op jit(solution)/shard_map/ppermute | solution.py:35
  164.9 11.3 %collective-permute-start.40 = (bf16[128,2048]{1,0:T(8,128)(2,1)S(1)}, bf16[128,2048]{1,0:T(8,128)(2,1)S(1)}, u32[]{:S(2)}, u32[]{:S(2)}) collective-permute-start(bf16[128,2048]{1,0:T(8,128)(2,1)S(1)} %add_convert_fusion), channel_id=1, source_target_pairs={{0,16},{4,20},{16,24},{20,28},{24,8},{28,12},{8,0},{12,4},{1,17},{... | collective-permute-start | bytes 1572872 | tf_op jit(solution)/shard_map/ppermute | solution.py:35
  (28 other events, 270.0 us)
where the time goes:
time: 178 us
  waiting for transfers between devices  86 us (48%)
  starting transfers between devices  47.8 us (27%)
  Pallas kernels  14.7 us (8%)
  other arithmetic  12.8 us (7%)
  matrix products  7.56 us (4%)
  blocking collectives  6.31 us (4%)
  local copies, waits for them, and re-layouts  2.31 us (1%)
    ppermute x31, waiting for transfers between devices, swapped(): lax.ppermute(block, axis, [(i, i ^ bit) for i in range(lax.axis_size(axis...  63 us
    ppermute x31, starting transfers between devices, swapped(): lax.ppermute(block, axis, [(i, i ^ bit) for i in range(lax.axis_size(axis...  26.2 us
    ppermute x9, waiting for transfers between devices, around(): return lax.ppermute(block, 'sp', route)  22.9 us
    ppermute x9, starting transfers between devices, around(): return lax.ppermute(block, 'sp', route)  16.7 us
    pallas_call x4, Pallas kernels, expert_step(): pl.pallas_call(expert_kernel, out_shape=(jax.ShapeDtypeStruct((rows // 2,...  14.7 us
    dot_general x20, matrix products, matmul(): return jnp.dot(a, b, preferred_element_type=jnp.float32)  7.56 us
    psum x1, blocking collectives, convolve(): lax.psum((jnp.sum(convolved, axis=1), jnp.sum(convolved * convolved, axis...  6.31 us
    reduce_sum x1, other arithmetic, convolve(): jnp.sum(convolved, axis=1)  5.05 us
  transfers between devices with their start and end apart: 41, of which 24 were waited for; matrix products, arithmetic and copies ran while one was open for 8% of the time, Pallas kernels for 8%

commit v1 on v0

--- a/solution.py
+++ b/solution.py
@@ -51,85 +51,227 @@
     return ((upper + 1.0) * gated * jax.nn.sigmoid(SLOPE * gated)).astype(jnp.bfloat16)
 
 
-def expert_kernel(near, far, gate_matrix, up_matrix, down_matrix, keep, pass_on, send):
-    def product(tokens):
-        gated = jnp.minimum(matmul(tokens, gate_matrix[...]), LIMIT)
-        upper = jnp.clip(matmul(tokens, up_matrix[...]), -LIMIT, LIMIT)
-        activity = (upper + 1.0) * gated / (1.0 + jnp.exp(-SLOPE * gated))
-        return matmul(activity.astype(jnp.bfloat16), down_matrix[...])
-
-    send[...] = product(far[...]).astype(jnp.bfloat16)
-    sums = product(near[...])
-    half = keep.shape[0]
-    keep[...] = sums[:half]
-    pass_on[...] = sums[half:]
-
-
-def expert_step(near, far, gate_matrix, up_matrix, down_matrix):
-    rows, width = near.shape
+def expert_kernel(tokens, gate_matrix, up_matrix, down_matrix, *outs):
+    gated = jnp.minimum(matmul(tokens[...], gate_matrix[...]), LIMIT)
+    upper = jnp.clip(matmul(tokens[...], up_matrix[...]), -LIMIT, LIMIT)
+    activity = (upper + 1.0) * gated / (1.0 + jnp.exp(-SLOPE * gated))
+    sums = matmul(activity.astype(jnp.bfloat16), down_matrix[...])
+    rows = sums.shape[0] // len(outs)
+    for i, out in enumerate(outs):
+        out[...] = sums[i * rows : (i + 1) * rows].astype(out.dtype)
+
+
+def expert_step(tokens, gate_matrix, up_matrix, down_matrix, dtype, parts):
+    rows, width = tokens.shape
     vmem = pl.BlockSpec(memory_space=pltpu.VMEM)
     return pl.pallas_call(
         expert_kernel,
-        out_shape=(
-            jax.ShapeDtypeStruct((rows // 2, width), jnp.float32),
-            jax.ShapeDtypeStruct((rows // 2, width), jnp.float32),
-            jax.ShapeDtypeStruct((rows, width), jnp.bfloat16),
-        ),
-        in_specs=[vmem] * 5,
-        out_specs=(vmem,) * 3,
-        compiler_params=pltpu.CompilerParams(vmem_limit_bytes=40 * 2**20),
+        out_shape=(jax.ShapeDtypeStruct((rows // parts, width), dtype),) * parts,
+        in_specs=[vmem] * 4,
+        out_specs=(vmem,) * parts,
+        compiler_params=pltpu.CompilerParams(vmem_limit_bytes=16 * 2**20),
         cost_estimate=pl.CostEstimate(
-            flops=12 * rows * width * gate_matrix.shape[1], transcendentals=0, bytes_accessed=0
+            flops=6 * rows * width * gate_matrix.shape[1], transcendentals=0, bytes_accessed=0
         ),
         name="expert_step",
-    )(near, far, gate_matrix, up_matrix, down_matrix)
+    )(tokens, gate_matrix, up_matrix, down_matrix)
 
 
 def gated_rows(value, gate):
     return (value.astype(jnp.float32) * jax.nn.sigmoid(gate.astype(jnp.float32))).astype(jnp.bfloat16)
 
 
-def convolve(glu_value, glu_gate, conv_kernel, norm_gain):
-    reach_back = conv_kernel.shape[0] - 1
+def convolve_rows(extended, taps, first, row, rows, window):
+    lanes = window.stop - window.start
+    sums = jnp.zeros((rows, lanes), jnp.float32)
+    for shift in range(8):
+        part = jnp.zeros(((rows + 8) // 8, 8, lanes), jnp.float32)
+        for k in range(taps.shape[0]):
+            if (first + k) % 8 == shift:
+                block = extended[pl.ds(row + first + k - shift, rows + 8), window]
+                tap = jnp.broadcast_to(taps[k : k + 1, window], (8, lanes))
+                part = part + block.reshape(part.shape) * tap[None]
+        sums = sums + part.reshape(rows + 8, lanes)[shift : shift + rows]
+    return sums
+
+
+def convolve_kernel(gated, kernel, gain, weight, out, total, squares, taps, gains, weights, extended, arrived, *, pad, rows):
+    length, channels = gated.shape
+    moves = [
+        pltpu.make_async_copy(source, target, arrived.at[i])
+        for i, (source, target) in enumerate(((kernel, taps), (gain, gains), (weight, weights)))
+    ]
+    for move in moves:
+        move.start()
+    extended[pl.ds(0, pad), :] = jnp.zeros((pad, channels), jnp.float32)
+    extended[pl.ds(pad, length), :] = gated[...].astype(jnp.float32)
+    moves[0].wait()
+    first = pad - (taps.shape[0] - 1)
+
+    def body(i, carry):
+        row = pl.multiple_of(i * rows, rows)
+        own_total = jnp.zeros((rows, 128), jnp.float32)
+        own_squares = jnp.zeros((rows, 128), jnp.float32)
+        for lane in range(0, channels, 128):
+            window = slice(lane, lane + 128)
+            sums = convolve_rows(extended, taps, first, row, rows, window)
+            out[pl.ds(row, rows), window] = sums
+            own_total = own_total + sums
+            own_squares = own_squares + sums * sums
+        total[pl.ds(row, rows), :] = own_total
+        squares[pl.ds(row, rows), :] = own_squares
+        return carry
+
+    lax.fori_loop(0, length // rows, body, 0)
+    moves[1].wait()
+    moves[2].wait()
+
+
+def head_kernel(before, gated, taps, total, squares, head, stats, extended):
+    pad, channels = before.shape
+    first = pad - (taps.shape[0] - 1)
+    extended[0:pad, :] = before[...].astype(jnp.float32)
+    extended[pad : 2 * pad, :] = gated[0:pad, :].astype(jnp.float32)
+    total[0:pad, :] = jnp.zeros((pad, 128), jnp.float32)
+    squares[0:pad, :] = jnp.zeros((pad, 128), jnp.float32)
+    for lane in range(0, channels, 128):
+        window = slice(lane, lane + 128)
+        sums = convolve_rows(extended, taps, first, 0, pad, window)
+        head[:, window] = sums
+        total[0:pad, :] += sums
+        squares[0:pad, :] += sums * sums
+    ones = jnp.ones((8, 128), jnp.float32)
+    for place, partial in enumerate((total, squares)):
+        sums = lax.dot_general(
+            ones,
+            partial[...],
+            (((1,), (1,)), ((), ())),
+            precision=lax.Precision.HIGHEST,
+            preferred_element_type=jnp.float32,
+        )
+        stats[place : place + 1, :] = sums[:1]
+
+
+def in_vmem(*arrays):
+    return tuple(pltpu.with_memory_space_constraint(a, pltpu.VMEM) for a in arrays)
+
+
+def convolve(glu_value, glu_gate, conv_kernel, norm_gain, mix_weight):
     length, channels = glu_value.shape
-    tail = slice(length - reach_back, length)
+    rows = min(128, length)
+    pad = -(-(conv_kernel.shape[0] - 1) // 16) * 16
+    tail = slice(length - pad, length)
     before_rows = shifted(gated_rows(glu_value[tail], glu_gate[tail]), "sp", 1)
-    gated_in = gated_rows(glu_value, glu_gate)
-    extended = jnp.concatenate([before_rows, gated_in], axis=0).astype(jnp.float32)
-    convolved = jnp.zeros(gated_in.shape, jnp.float32)
-    for offset in range(reach_back + 1):
-        convolved = convolved + conv_kernel[offset] * extended[offset : offset + length]
-    channel_sum, squares = lax.psum(
-        (jnp.sum(convolved, axis=1), jnp.sum(convolved * convolved, axis=1)), "tp"
+    gated = gated_rows(glu_value, glu_gate)
+    norm_gain = norm_gain[None]
+    vmem, hbm = pl.BlockSpec(memory_space=pltpu.VMEM), pl.BlockSpec(memory_space=pltpu.HBM)
+    convolved, total, squares, taps, gains, weights = pl.pallas_call(
+        lambda *refs: convolve_kernel(*refs, pad=pad, rows=rows),
+        out_shape=(
+            jax.ShapeDtypeStruct((length, channels), jnp.float32),
+            pltpu.VMEM((length, 128), jnp.float32),
+            pltpu.VMEM((length, 128), jnp.float32),
+            pltpu.VMEM(conv_kernel.shape, jnp.float32),
+            pltpu.VMEM(norm_gain.shape, jnp.float32),
+            pltpu.VMEM(mix_weight.shape, mix_weight.dtype),
+        ),
+        in_specs=[vmem, hbm, hbm, hbm],
+        out_specs=(vmem,) * 6,
+        scratch_shapes=[
+            pltpu.VMEM((length + pad + 8, channels), jnp.float32),
+            pltpu.SemaphoreType.DMA((3,)),
+        ],
+        compiler_params=pltpu.CompilerParams(vmem_limit_bytes=16 * 2**20),
+        name="convolve",
+    )(*in_vmem(gated), *(pltpu.with_memory_space_constraint(a, pltpu.HBM) for a in (conv_kernel, norm_gain, mix_weight)))
+    head, own = pl.pallas_call(
+        head_kernel,
+        out_shape=(pltpu.VMEM((pad, channels), jnp.float32), pltpu.VMEM((2, length), jnp.float32)),
+        in_specs=[vmem] * 5,
+        out_specs=(vmem,) * 2,
+        scratch_shapes=[pltpu.VMEM((2 * pad + 8, channels), jnp.float32)],
+        compiler_params=pltpu.CompilerParams(vmem_limit_bytes=8 * 2**20),
+        name="head",
+    )(*in_vmem(before_rows, gated, taps, total, squares))
+    stats = [own] + [swapped(own, "tp", d) for d in range(1, lax.axis_size("tp"))]
+    return convolved, head, stats, gains, weights
+
+
+def first_products_kernel(here, convolved, head, gain, mix_weight, *refs, bit, far, shares):
+    stats, (mix_in, send, keep, wide) = refs[:shares], refs[shares:]
+    rows, channels = send.shape[0], convolved.shape[1] * shares
+    sums = stats[0][...]
+    for share in stats[1:]:
+        sums = sums + share[...]
+    centre = sums[0:1] / channels
+    spread = sums[1:2] / channels - centre * centre
+    wide[...] = jnp.zeros_like(wide)
+    wide[0:1, :] = centre
+    wide[1:2, :] = lax.rsqrt(spread + EPSILON)
+    place = lax.broadcasted_iota(jnp.int32, (wide.shape[0], 128), 0)
+    centre, scale = (
+        lax.dot_general(
+            wide[...],
+            (place == i).astype(jnp.float32),
+            (((0,), (0,)), ((), ())),
+            precision=lax.Precision.HIGHEST,
+            preferred_element_type=jnp.float32,
+        )
+        for i in (0, 1)
     )
-    channels = channels * lax.axis_size("tp")
-    centre = channel_sum / channels
-    spread = squares / channels - centre * centre
-    normed = (convolved - centre[:, None]) * lax.rsqrt(spread[:, None] + EPSILON) * norm_gain
-    return jax.nn.silu(normed).astype(jnp.bfloat16)
-
-
-def scattered_product(mix_in, mix_weight):
+    for lane in range(0, convolved.shape[1], 128):
+        window = slice(lane, lane + 128)
+        values = jnp.concatenate([head[:, window], convolved[head.shape[0] :, window]], axis=0)
+        normed = (values - centre) * scale * gain[:, window]
+        mix_in[:, window] = (normed / (1.0 + jnp.exp(-normed))).astype(jnp.bfloat16)
+    for d, out in ((far + bit, send), (far, keep)):
+        own = mix_in[pl.ds(pl.multiple_of((here[0] ^ d) * rows, rows), rows), :]
+        out[...] = matmul(own, mix_weight[...]).astype(out.dtype)
+
+
+def last_products_kernel(here, mix_in, mix_weight, send, keep, *, bit):
+    rows = send.shape[0]
+    for d, out in ((bit, send), (0, keep)):
+        own = mix_in[pl.ds(pl.multiple_of((here[0] ^ d) * rows, rows), rows), :]
+        out[...] = matmul(own, mix_weight[...]).astype(out.dtype)
+
+
+def scattered_product(convolved, head, stats, norm_gain, mix_weight):
     count = lax.axis_size("tp")
-    rows = mix_in.shape[0] // count
-    here = lax.axis_index("tp")
-
-    def product(d):
-        own = lax.dynamic_slice_in_dim(mix_in, (here ^ d) * rows, rows, axis=0)
-        return matmul(own, mix_weight)
-
-    parts = [None] * count
-    for d in reversed(range(count)):
-        parts[d] = product(d)
-    bit = 1
-    while bit < count:
-        kept = {}
-        for d in reversed(range(0, count, 2 * bit)):
-            arrived = swapped(parts[d + bit].astype(jnp.bfloat16), "tp", bit)
-            kept[d] = parts[d] + arrived.astype(jnp.float32)
-        parts = [kept.get(d) for d in range(count)]
-        bit *= 2
-    return parts[0]
+    assert count == 4
+    rows, width = convolved.shape[0] // count, mix_weight.shape[1]
+    here = lax.axis_index("tp").reshape(1).astype(jnp.int32)
+    vmem, smem = pl.BlockSpec(memory_space=pltpu.VMEM), pl.BlockSpec(memory_space=pltpu.SMEM)
+    products = (pltpu.VMEM((rows, width), jnp.bfloat16), pltpu.VMEM((rows, width), jnp.float32))
+    params = pltpu.CompilerParams(vmem_limit_bytes=8 * 2**20)
+    mix_in, far_send, far_keep = pl.pallas_call(
+        lambda *refs: first_products_kernel(*refs, bit=1, far=2, shares=count),
+        out_shape=(pltpu.VMEM(convolved.shape, jnp.bfloat16),) + products,
+        in_specs=[smem] + [vmem] * (4 + count),
+        out_specs=(vmem,) * 3,
+        scratch_shapes=[pltpu.VMEM((8, convolved.shape[0]), jnp.float32)],
+        compiler_params=params,
+        name="first_products",
+    )(here, convolved, *in_vmem(head, norm_gain, mix_weight, *stats))
+    arrived = swapped(far_send, "tp", 1)
+    far_sum = (far_keep + arrived.astype(jnp.float32)).astype(jnp.bfloat16)
+    from_chip = swapped(far_sum, "tp", 2)
+    near_send, near_keep = pl.pallas_call(
+        lambda *refs: last_products_kernel(*refs, bit=1),
+        out_shape=products,
+        in_specs=[smem, vmem, vmem],
+        out_specs=(vmem,) * 2,
+        compiler_params=params,
+        name="last_products",
+    )(here, *in_vmem(mix_in, mix_weight))
+    arrived = swapped(near_send, "tp", 1)
+    return near_keep, arrived, from_chip
+
+
+def hidden_kernel(residual, keep, from_core, from_chip, gain, out):
+    values = residual[...].astype(jnp.float32) + keep[...]
+    values = values + from_core[...].astype(jnp.float32) + from_chip[...].astype(jnp.float32)
+    out[...] = normalize(values, gain[...]).astype(out.dtype)
 
 
 def slots_of(ids, weights, expert, capacity):
@@ -167,18 +309,25 @@
         picked = matmul(own_hot.T, block).astype(jnp.bfloat16)
         own_x = swapped(picked, "tp", 2)
         far_x = swapped(arrived, "tp", 2)
-        near = jnp.concatenate([picked, arrived, own_x, far_x], axis=0)
+        near = jnp.concatenate([arrived, far_x, picked, own_x], axis=0)
         far = swapped(near, "tp", 1)
-        keep, pass_on, send = expert_step(near, far, gate_local, up_local, down_local)
-        from_core = swapped(send, "tp", 1)
-        half = keep.shape[0]
-        pass_on = (pass_on + from_core[half:].astype(jnp.float32)).astype(jnp.bfloat16)
-        from_chip = swapped(pass_on, "tp", 2)
-        sums = keep + from_core[:half].astype(jnp.float32) + from_chip.astype(jnp.float32)
-        sums = sums.astype(jnp.bfloat16)
-        mine, theirs = sums[:capacity], sums[capacity:]
-        theirs = swapped(theirs, "sp", 1)
-        share = own_weight[:, None] * matmul(own_hot, mine) + far_weight[:, None] * matmul(far_hot, theirs)
+        near_sums = expert_step(near, gate_local, up_local, down_local, jnp.float32, 4)
+        far_sums = expert_step(far, gate_local, up_local, down_local, jnp.bfloat16, 2)
+
+        def crossed(send, leave):
+            from_core = swapped(send, "tp", 1)
+            leave = leave + from_core[capacity:].astype(jnp.float32)
+            return from_core[:capacity], swapped(leave.astype(jnp.bfloat16), "tp", 2)
+
+        def summed(keep, from_core, from_chip):
+            total = keep + from_core.astype(jnp.float32) + from_chip.astype(jnp.float32)
+            return total.astype(jnp.bfloat16)
+
+        theirs = crossed(far_sums[0], near_sums[1])
+        mine = crossed(far_sums[1], near_sums[3])
+        far_sum = swapped(summed(near_sums[0], *theirs), "sp", 1)
+        own_sum = summed(near_sums[2], *mine)
+        share = own_weight[:, None] * matmul(own_hot, own_sum) + far_weight[:, None] * matmul(far_hot, far_sum)
         if s == 0:
             own_share = share
         else:
@@ -236,10 +385,17 @@
     w_down,
     out_gain,
 ):
-    mix_in = convolve(glu_value, glu_gate, conv_kernel, norm_gain)
-    mix_in, expert_ids, route_weight = lax.optimization_barrier((mix_in, expert_ids, route_weight))
-    mixed_rows = scattered_product(mix_in, mix_weight)
-    hidden = normalize(residual.astype(jnp.float32) + mixed_rows, resid_gain).astype(jnp.bfloat16)
+    convolved, head, stats, gains, weights = convolve(glu_value, glu_gate, conv_kernel, norm_gain, mix_weight)
+    mixed_rows = scattered_product(convolved, head, stats, gains, weights)
+    vmem = pl.BlockSpec(memory_space=pltpu.VMEM)
+    hidden = pl.pallas_call(
+        hidden_kernel,
+        out_shape=jax.ShapeDtypeStruct(residual.shape, jnp.bfloat16),
+        in_specs=[vmem] * 5,
+        out_specs=vmem,
+        compiler_params=pltpu.CompilerParams(vmem_limit_bytes=8 * 2**20),
+        name="hidden",
+    )(residual, *mixed_rows, resid_gain[None])
     experts = lax.axis_size("sp")
     own_count, top_count = expert_ids.shape
     capacity = 2 * own_count * top_count // experts

time: 178 us -> 189 us (1.062)
  waiting for transfers between devices: 86 us -> 100 us
  Pallas kernels: 14.7 us -> 22.7 us
  blocking collectives: 6.31 us -> 0 us
  other arithmetic: 12.8 us -> 8.05 us
  starting transfers between devices: 47.8 us -> 50.6 us
  local copies, waits for them, and re-layouts: 2.31 us -> 0.03 us
    ppermute x31 -> x42, waiting for transfers between devices: 63 us -> 76.9 us  [swapped(): lax.ppermute(block, axis, [(i, i ^ bit) for i in range(lax.axis_size(axis...]
    pallas_call x4 -> x13, Pallas kernels: 14.7 us -> 22.7 us  [the longest x8 15.3 us: expert_step(): pl.pallas_call(expert_kernel, out_shape=(jax.ShapeDtypeStruct((rows // pa...]
    psum x1 -> x0, blocking collectives: 6.31 us -> none  [convolve(): lax.psum((jnp.sum(convolved, axis=1), jnp.sum(convolved * convolved, axis...]
    reduce_sum x2 -> x0, other arithmetic: 5.45 us -> none  [the longest x1 5.05 us: convolve(): jnp.sum(convolved, axis=1)]
    ppermute x31 -> x42, starting transfers between devices: 26.2 us -> 31.4 us  [swapped(): lax.ppermute(block, axis, [(i, i ^ bit) for i in range(lax.axis_size(axis...]
    slice x6 -> x0, local copies, waits for them, and re-layouts: 2.25 us -> none  [the longest x2 2.17 us: convolve(): conv_kernel[offset] * extended[offset:offset + length]]
    dot_general x20 -> x16, matrix products: 7.56 us -> 5.82 us  [matmul(): return jnp.dot(a, b, preferred_element_type=jnp.float32)]
  transfers between devices with their start and end apart: 41 -> 52, of which waited for: 24 -> 27; matrix products, arithmetic and copies ran while one was open for 8% -> 6% of each run, Pallas kernels for 8% -> 12%
where the time goes in v1:
time: 189 us; the launch traced here: 188 us
  waiting for transfers between devices  100 us (53%)
  starting transfers between devices  50.6 us (27%)
  Pallas kernels  22.7 us (12%)
  other arithmetic  8.05 us (4%)
  matrix products  5.82 us (3%)
    ppermute x42, waiting for transfers between devices, swapped(): lax.ppermute(block, axis, [(i, i ^ bit) for i in range(lax.axis_size(axis...  76.9 us
    ppermute x42, starting transfers between devices, swapped(): lax.ppermute(block, axis, [(i, i ^ bit) for i in range(lax.axis_size(axis...  31.4 us
    ppermute x9, waiting for transfers between devices, around(): return lax.ppermute(block, 'sp', route)  23.5 us
    ppermute x9, starting transfers between devices, around(): return lax.ppermute(block, 'sp', route)  15.8 us
    pallas_call x8, Pallas kernels, expert_step(): pl.pallas_call(expert_kernel, out_shape=(jax.ShapeDtypeStruct((rows // pa...  15.3 us
    dot_general x16, matrix products, matmul(): return jnp.dot(a, b, preferred_element_type=jnp.float32)  5.82 us
    pallas_call x1, Pallas kernels, convolve(): pl.pallas_call(lambda *refs: convolve_kernel(*refs, pad=pad, rows=rows),...  3.79 us
  transfers between devices with their start and end apart: 52, of which 27 were waited for; matrix products, arithmetic and copies ran while one was open for 6% of the time, Pallas kernels for 12%

profile of v1, /device:TPU:0, one launch (start us, length us, event | category | flops | bytes accessed | tf_op | source)
XLA Modules:
  0.0 188.3 jit_solution(4003764409467105935)
XLA Ops:
  1.4 3.1 %collective-permute-start.40 = (f32[128,4]{0,1:T(4,128)S(1)}, f32[128,4]{0,1:T(4,128)S(1)}, u32[]{:S(2)}, u32[]{:S(2)}) collective-permute-start(f32[128,4]{0,1:T(4,128)S(1)} %pad_maximum_fusion.4), channel_id=1, source_target_pairs={{0,8},{4,12},{16,0},{20,4},{24,16},{28,20},{8,24},{12,28},{1,9},{5... | collective-permute-start | bytes 6152 | tf_op jit(solution)/shard_map/ppermute | solution.py:35
  4.4 2.5 %collective-permute-start.28 = (f32[128,4]{0,1:T(4,128)S(1)}, f32[128,4]{0,1:T(4,128)S(1)}, u32[]{:S(2)}, u32[]{:S(2)}) collective-permute-start(f32[128,4]{0,1:T(4,128)S(1)} %pad_maximum_fusion.4), channel_id=1, source_target_pairs={{0,24},{4,28},{16,8},{20,12},{24,0},{28,4},{8,16},{12,20},{1,25},{... | collective-permute-start | bytes 6152 | tf_op jit(solution)/shard_map/ppermute | solution.py:35
  9.3 3.4 %collective-permute-start = (bf16[32,512]{1,0:T(8,128)(2,1)S(1)}, bf16[32,512]{1,0:T(8,128)(2,1)S(1)}, u32[]{:S(2)}, u32[]{:S(2)}) collective-permute-start(bf16[32,512]{1,0:T(8,128)(2,1)S(1)} %multiply_convert_fusion.2), channel_id=1, source_target_pairs={{0,4},{4,8},{8,12},{12,16},{16,20},{20,24},{24,28},{1,5},{5,9},{9,... | collective-permute-start | bytes 98312 | tf_op jit(solution)/shard_map/ppermute | solution.py:17
  15.2 3.8 %convolve.1 = (f32[512,512]{1,0:T(8,128)S(1)}, f32[512,128]{1,0:T(8,128)S(1)}, f32[512,128]{1,0:T(8,128)S(1)}, f32[31,512]{1,0:T(8,128)S(1)}, f32[1,512]{1,0:T(1,128)S(1)}, /*index=5*/bf16[512,2048]{1,0:T(8,128)(2,1)S(1)}) custom-call(bf16[512,512]{1,0:T(8,128)(2,1)S(1)} %multiply_convert_fusion.1.refs_0_.gated, f32[31,512]{1,0:T(8,128)} %refs_1_.1, ...), custom_call_target="tpu_custom_call" | custom-call | tf_op jit(solution)/shard_map/convolve/pallas_call | solution.py:168
  29.5 13.0 %collective-permute-done.6.from_chip = bf16[128,2048]{1,0:T(8,128)(2,1)S(1)} collective-permute-done((bf16[128,2048]{1,0:T(8,128)(2,1)S(1)}, bf16[128,2048]{1,0:T(8,128)(2,1)S(1)}, u32[]{:S(2)}, u32[]{:S(2)}) %collective-permute-start.6) | collective-permute-done | bytes 524320 | tf_op jit(solution)/shard_map/ppermute | solution.py:21
  46.0 5.1 %collective-permute-done.7 = bf16[64,2048]{1,0:T(8,128)(2,1)S(1)} collective-permute-done((bf16[64,2048]{1,0:T(8,128)(2,1)S(1)}, bf16[64,2048]{1,0:T(8,128)(2,1)S(1)}, u32[]{:S(2)}, u32[]{:S(2)}) %collective-permute-start.7) | collective-permute-done | bytes 262176 | tf_op jit(solution)/shard_map/ppermute | solution.py:21
  51.6 4.7 %collective-permute-done.17 = bf16[128,2048]{1,0:T(8,128)(2,1)S(1)} collective-permute-done((bf16[128,2048]{1,0:T(8,128)(2,1)S(1)}, bf16[128,2048]{1,0:T(8,128)(2,1)S(1)}, u32[]{:S(2)}, u32[]{:S(2)}) %collective-permute-start.17) | collective-permute-done | bytes 524320 | tf_op jit(solution)/shard_map/ppermute | solution.py:35
  60.0 3.4 %collective-permute-done.18 = bf16[64,2048]{1,0:T(8,128)(2,1)S(1)} collective-permute-done((bf16[64,2048]{1,0:T(8,128)(2,1)S(1)}, bf16[64,2048]{1,0:T(8,128)(2,1)S(1)}, u32[]{:S(2)}, u32[]{:S(2)}) %collective-permute-start.18) | collective-permute-done | bytes 262176 | tf_op jit(solution)/shard_map/ppermute | solution.py:21
  65.9 3.8 %collective-permute-done.19 = bf16[64,2048]{1,0:T(8,128)(2,1)S(1)} collective-permute-done((bf16[64,2048]{1,0:T(8,128)(2,1)S(1)}, bf16[64,2048]{1,0:T(8,128)(2,1)S(1)}, u32[]{:S(2)}, u32[]{:S(2)}) %collective-permute-start.19) | collective-permute-done | bytes 262176 | tf_op jit(solution)/shard_map/ppermute | solution.py:21
  69.8 2.7 %collective-permute-start.41 = (bf16[128,2048]{1,0:T(8,128)(2,1)S(1)}, bf16[128,2048]{1,0:T(8,128)(2,1)S(1)}, u32[]{:S(2)}, u32[]{:S(2)}) collective-permute-start(bf16[128,2048]{1,0:T(8,128)(2,1)S(1)} %collective-permute-done.29), channel_id=1, source_target_pairs={{0,16},{4,20},{16,24},{20,28},{24,8},{28,12},{8,0},{12,4},{1,17},{... | collective-permute-start | bytes 1572872 | tf_op jit(solution)/shard_map/ppermute | solution.py:35
  81.5 2.8 %collective-permute-start.42 = (bf16[64,2048]{1,0:T(8,128)(2,1)S(1)}, bf16[64,2048]{1,0:T(8,128)(2,1)S(1)}, u32[]{:S(2)}, u32[]{:S(2)}) collective-permute-start(bf16[64,2048]{1,0:T(8,128)(2,1)S(1)} %convolution_convert_fusion.1), channel_id=1, source_target_pairs={{0,4},{4,0},{8,12},{12,8},{16,20},{20,16},{24,28},{28,24},{1,5},{5... | collective-permute-start | bytes 786440 | tf_op jit(solution)/shard_map/ppermute | solution.py:21
  93.2 3.5 %collective-permute-done.44 = bf16[64,2048]{1,0:T(8,128)(2,1)S(1)} collective-permute-done((bf16[64,2048]{1,0:T(8,128)(2,1)S(1)}, bf16[64,2048]{1,0:T(8,128)(2,1)S(1)}, u32[]{:S(2)}, u32[]{:S(2)}) %collective-permute-start.44) | collective-permute-done | bytes 262176 | tf_op jit(solution)/shard_map/ppermute | solution.py:21
  96.8 5.1 %collective-permute-done.43 = bf16[64,2048]{1,0:T(8,128)(2,1)S(1)} collective-permute-done((bf16[64,2048]{1,0:T(8,128)(2,1)S(1)}, bf16[64,2048]{1,0:T(8,128)(2,1)S(1)}, u32[]{:S(2)}, u32[]{:S(2)}) %collective-permute-start.43) | collective-permute-done | bytes 262176 | tf_op jit(solution)/shard_map/ppermute | solution.py:21
  107.9 3.0 %collective-permute-done.14 = bf16[64,2048]{1,0:T(8,128)(2,1)S(1)} collective-permute-done((bf16[64,2048]{1,0:T(8,128)(2,1)S(1)}, bf16[64,2048]{1,0:T(8,128)(2,1)S(1)}, u32[]{:S(2)}, u32[]{:S(2)}) %collective-permute-start.14) | collective-permute-done | bytes 262176 | tf_op jit(solution)/shard_map/ppermute | solution.py:21
  116.2 6.9 %collective-permute-done.25 = bf16[64,2048]{1,0:T(8,128)(2,1)S(1)} collective-permute-done((bf16[64,2048]{1,0:T(8,128)(2,1)S(1)}, bf16[64,2048]{1,0:T(8,128)(2,1)S(1)}, u32[]{:S(2)}, u32[]{:S(2)}) %collective-permute-start.25) | collective-permute-done | bytes 262176 | tf_op jit(solution)/shard_map/ppermute | solution.py:21
  124.7 6.0 %collective-permute-done.23 = bf16[64,2048]{1,0:T(8,128)(2,1)S(1)} collective-permute-done((bf16[64,2048]{1,0:T(8,128)(2,1)S(1)}, bf16[64,2048]{1,0:T(8,128)(2,1)S(1)}, u32[]{:S(2)}, u32[]{:S(2)}) %collective-permute-start.23) | collective-permute-done | bytes 262176 | tf_op jit(solution)/shard_map/ppermute | solution.py:21
  136.6 3.2 %collective-permute-done.26 = bf16[64,2048]{1,0:T(8,128)(2,1)S(1)} collective-permute-done((bf16[64,2048]{1,0:T(8,128)(2,1)S(1)}, bf16[64,2048]{1,0:T(8,128)(2,1)S(1)}, u32[]{:S(2)}, u32[]{:S(2)}) %collective-permute-start.26) | collective-permute-done | bytes 262176 | tf_op jit(solution)/shard_map/ppermute | solution.py:21
  140.2 6.4 %collective-permute-done.37 = bf16[64,2048]{1,0:T(8,128)(2,1)S(1)} collective-permute-done((bf16[64,2048]{1,0:T(8,128)(2,1)S(1)}, bf16[64,2048]{1,0:T(8,128)(2,1)S(1)}, u32[]{:S(2)}, u32[]{:S(2)}) %collective-permute-start.37) | collective-permute-done | bytes 262176 | tf_op jit(solution)/shard_map/ppermute | solution.py:21
  150.3 9.4 %collective-permute-done.27 = bf16[128,2048]{1,0:T(8,128)(2,1)S(1)} collective-permute-done((bf16[128,2048]{1,0:T(8,128)(2,1)S(1)}, bf16[128,2048]{1,0:T(8,128)(2,1)S(1)}, u32[]{:S(2)}, u32[]{:S(2)}) %collective-permute-start.27) | collective-permute-done | bytes 524320 | tf_op jit(solution)/shard_map/ppermute | solution.py:35
  162.9 3.4 %collective-permute-done.49 = bf16[64,2048]{1,0:T(8,128)(2,1)S(1)} collective-permute-done((bf16[64,2048]{1,0:T(8,128)(2,1)S(1)}, bf16[64,2048]{1,0:T(8,128)(2,1)S(1)}, u32[]{:S(2)}, u32[]{:S(2)}) %collective-permute-start.49) | collective-permute-done | bytes 262176 | tf_op jit(solution)/shard_map/ppermute | solution.py:21
  167.8 5.8 %collective-permute-done.39 = bf16[128,2048]{1,0:T(8,128)(2,1)S(1)} collective-permute-done((bf16[128,2048]{1,0:T(8,128)(2,1)S(1)}, bf16[128,2048]{1,0:T(8,128)(2,1)S(1)}, u32[]{:S(2)}, u32[]{:S(2)}) %collective-permute-start.39) | collective-permute-done | bytes 524320 | tf_op jit(solution)/shard_map/ppermute | solution.py:35
  174.1 2.4 %collective-permute-start.51 = (bf16[128,2048]{1,0:T(8,128)(2,1)S(1)}, bf16[128,2048]{1,0:T(8,128)(2,1)S(1)}, u32[]{:S(2)}, u32[]{:S(2)}) collective-permute-start(bf16[128,2048]{1,0:T(8,128)(2,1)S(1)} %add_convert_fusion), channel_id=1, source_target_pairs={{0,16},{4,20},{16,24},{20,28},{24,8},{28,12},{8,0},{12,4},{1,17},{... | collective-permute-start | bytes 1572872 | tf_op jit(solution)/shard_map/ppermute | solution.py:35
  177.4 5.6 %collective-permute-done.12 = bf16[64,2048]{1,0:T(8,128)(2,1)S(1)} collective-permute-done((bf16[64,2048]{1,0:T(8,128)(2,1)S(1)}, bf16[64,2048]{1,0:T(8,128)(2,1)S(1)}, u32[]{:S(2)}, u32[]{:S(2)}) %collective-permute-start.12) | collective-permute-done | bytes 262176 | tf_op jit(solution)/shard_map/ppermute | solution.py:21
  183.0 3.4 %collective-permute-done.51 = bf16[128,2048]{1,0:T(8,128)(2,1)S(1)} collective-permute-done((bf16[128,2048]{1,0:T(8,128)(2,1)S(1)}, bf16[128,2048]{1,0:T(8,128)(2,1)S(1)}, u32[]{:S(2)}, u32[]{:S(2)}) %collective-permute-start.51) | collective-permute-done | bytes 524320 | tf_op jit(solution)/shard_map/ppermute | solution.py:35
  (167 shorter events, 75.2 us)
Async XLA Ops:
  1.4 17.6 %collective-permute-start.40 = (f32[128,4]{0,1:T(4,128)S(1)}, f32[128,4]{0,1:T(4,128)S(1)}, u32[]{:S(2)}, u32[]{:S(2)}) collective-permute-start(f32[128,4]{0,1:T(4,128)S(1)} %pad_maximum_fusion.4), channel_id=1, source_target_pairs={{0,8},{4,12},{16,0},{20,4},{24,16},{28,20},{8,24},{12,28},{1,9},{5... | collective-permute-start | bytes 6152 | tf_op jit(solution)/shard_map/ppermute | solution.py:35
  4.4 14.9 %collective-permute-start.28 = (f32[128,4]{0,1:T(4,128)S(1)}, f32[128,4]{0,1:T(4,128)S(1)}, u32[]{:S(2)}, u32[]{:S(2)}) collective-permute-start(f32[128,4]{0,1:T(4,128)S(1)} %pad_maximum_fusion.4), channel_id=1, source_target_pairs={{0,24},{4,28},{16,8},{20,12},{24,0},{28,4},{8,16},{12,20},{1,25},{... | collective-permute-start | bytes 6152 | tf_op jit(solution)/shard_map/ppermute | solution.py:35
  6.9 22.2 %collective-permute-start.16 = (f32[128,4]{0,1:T(4,128)S(1)}, f32[128,4]{0,1:T(4,128)S(1)}, u32[]{:S(2)}, u32[]{:S(2)}) collective-permute-start(f32[128,4]{0,1:T(4,128)S(1)} %pad_maximum_fusion.4), channel_id=1, source_target_pairs={{0,16},{4,20},{16,24},{20,28},{24,8},{28,12},{8,0},{12,4},{1,17},{... | collective-permute-start | bytes 6152 | tf_op jit(solution)/shard_map/ppermute | solution.py:35
  28.4 14.1 %collective-permute-start.6 = (bf16[128,2048]{1,0:T(8,128)(2,1)S(1)}, bf16[128,2048]{1,0:T(8,128)(2,1)S(1)}, u32[]{:S(2)}, u32[]{:S(2)}) collective-permute-start(bf16[128,2048]{1,0:T(8,128)(2,1)S(1)} %add_convert_fusion.3), channel_id=1, source_target_pairs={{0,2},{1,3},{2,0},{3,1},{4,6},{5,7},{6,4},{7,5},{8,10},{9,11},{10,... | collective-permute-start | bytes 1572872 | tf_op jit(solution)/shard_map/ppermute | solution.py:21
  43.0 13.2 %collective-permute-start.17 = (bf16[128,2048]{1,0:T(8,128)(2,1)S(1)}, bf16[128,2048]{1,0:T(8,128)(2,1)S(1)}, u32[]{:S(2)}, u32[]{:S(2)}) collective-permute-start(bf16[128,2048]{1,0:T(8,128)(2,1)S(1)} %hidden.1), channel_id=1, source_target_pairs={{0,16},{4,20},{16,24},{20,28},{24,8},{28,12},{8,0},{12,4},{1,17},{... | collective-permute-start | bytes 1572872 | tf_op jit(solution)/shard_map/ppermute | solution.py:35
  45.4 18.4 %collective-permute-start.9 = (bf16[64,2048]{1,0:T(8,128)(2,1)S(1)}, bf16[64,2048]{1,0:T(8,128)(2,1)S(1)}, u32[]{:S(2)}, u32[]{:S(2)}) collective-permute-start(bf16[64,2048]{1,0:T(8,128)(2,1)S(1)} %convolution_convert_fusion.6), channel_id=1, source_target_pairs={{0,2},{1,3},{2,0},{3,1},{4,6},{5,7},{6,4},{7,5},{8,10},{9,11},{10,... | collective-permute-start | bytes 786440 | tf_op jit(solution)/shard_map/ppermute | solution.py:21
  51.1 12.7 %collective-permute-start.8 = (bf16[64,2048]{1,0:T(8,128)(2,1)S(1)}, bf16[64,2048]{1,0:T(8,128)(2,1)S(1)}, u32[]{:S(2)}, u32[]{:S(2)}) collective-permute-start(bf16[64,2048]{1,0:T(8,128)(2,1)S(1)} %collective-permute-done.7), channel_id=1, source_target_pairs={{0,2},{1,3},{2,0},{3,1},{4,6},{5,7},{6,4},{7,5},{8,10},{9,11},{10,... | collective-permute-start | bytes 786440 | tf_op jit(solution)/shard_map/ppermute | solution.py:21
  63.9 20.7 %collective-permute-start.10 = (bf16[256,2048]{1,0:T(8,128)(2,1)S(1)}, bf16[256,2048]{1,0:T(8,128)(2,1)S(1)}, u32[]{:S(2)}, u32[]{:S(2)}) collective-permute-start(bf16[256,2048]{1,0:T(8,128)(2,1)S(1)} %pad_maximum_fusion.tokens), channel_id=1, source_target_pairs={{0,1},{1,0},{2,3},{3,2},{4,5},{5,4},{6,7},{7,6},{8,9},{9,8},{10,11... | collective-permute-start | bytes 3145736 | tf_op jit(solution)/shard_map/ppermute | solution.py:21
  75.9 28.0 %collective-permute-start.21 = (bf16[256,2048]{1,0:T(8,128)(2,1)S(1)}, bf16[256,2048]{1,0:T(8,128)(2,1)S(1)}, u32[]{:S(2)}, u32[]{:S(2)}) collective-permute-start(bf16[256,2048]{1,0:T(8,128)(2,1)S(1)} %pad_maximum_fusion.1.tokens), channel_id=1, source_target_pairs={{0,1},{1,0},{2,3},{3,2},{4,5},{5,4},{6,7},{7,6},{8,9},{9,8},{10,11... | collective-permute-start | bytes 3145736 | tf_op jit(solution)/shard_map/ppermute | solution.py:21
  84.6 12.1 %collective-permute-start.44 = (bf16[64,2048]{1,0:T(8,128)(2,1)S(1)}, bf16[64,2048]{1,0:T(8,128)(2,1)S(1)}, u32[]{:S(2)}, u32[]{:S(2)}) collective-permute-start(bf16[64,2048]{1,0:T(8,128)(2,1)S(1)} %convolution_convert_fusion), channel_id=1, source_target_pairs={{0,2},{1,3},{2,0},{3,1},{4,6},{5,7},{6,4},{7,5},{8,10},{9,11},{10,... | collective-permute-start | bytes 786440 | tf_op jit(solution)/shard_map/ppermute | solution.py:21
  87.2 14.9 %collective-permute-start.13 = (bf16[128,2048]{1,0:T(8,128)(2,1)S(1)}, bf16[128,2048]{1,0:T(8,128)(2,1)S(1)}, u32[]{:S(2)}, u32[]{:S(2)}) collective-permute-start(bf16[128,2048]{1,0:T(8,128)(2,1)S(1)} %get-tuple-element.59), channel_id=1, source_target_pairs={{0,1},{1,0},{2,3},{3,2},{4,5},{5,4},{6,7},{7,6},{8,9},{9,8},{10,11... | collective-permute-start | bytes 1572872 | tf_op jit(solution)/shard_map/ppermute | solution.py:21
  88.6 13.3 %collective-permute-start.43 = (bf16[64,2048]{1,0:T(8,128)(2,1)S(1)}, bf16[64,2048]{1,0:T(8,128)(2,1)S(1)}, u32[]{:S(2)}, u32[]{:S(2)}) collective-permute-start(bf16[64,2048]{1,0:T(8,128)(2,1)S(1)} %collective-permute-done.42), channel_id=1, source_target_pairs={{0,2},{1,3},{2,0},{3,1},{4,6},{5,7},{6,4},{7,5},{8,10},{9,11},{10,... | collective-permute-start | bytes 786440 | tf_op jit(solution)/shard_map/ppermute | solution.py:21
  91.2 19.8 %collective-permute-start.33 = (bf16[256,2048]{1,0:T(8,128)(2,1)S(1)}, bf16[256,2048]{1,0:T(8,128)(2,1)S(1)}, u32[]{:S(2)}, u32[]{:S(2)}) collective-permute-start(bf16[256,2048]{1,0:T(8,128)(2,1)S(1)} %pad_maximum_fusion.2.tokens), channel_id=1, source_target_pairs={{0,1},{1,0},{2,3},{3,2},{4,5},{5,4},{6,7},{7,6},{8,9},{9,8},{10,11... | collective-permute-start | bytes 3145736 | tf_op jit(solution)/shard_map/ppermute | solution.py:21
  96.8 79.7 %collective-permute-start.11 = (bf16[128,2048]{1,0:T(8,128)(2,1)S(1)}, bf16[128,2048]{1,0:T(8,128)(2,1)S(1)}, u32[]{:S(2)}, u32[]{:S(2)}) collective-permute-start(bf16[128,2048]{1,0:T(8,128)(2,1)S(1)} %get-tuple-element.56), channel_id=1, source_target_pairs={{0,1},{1,0},{2,3},{3,2},{4,5},{5,4},{6,7},{7,6},{8,9},{9,8},{10,11... | collective-permute-start | bytes 1572872 | tf_op jit(solution)/shard_map/ppermute | solution.py:21
  102.0 32.2 %collective-permute-start.45 = (bf16[256,2048]{1,0:T(8,128)(2,1)S(1)}, bf16[256,2048]{1,0:T(8,128)(2,1)S(1)}, u32[]{:S(2)}, u32[]{:S(2)}) collective-permute-start(bf16[256,2048]{1,0:T(8,128)(2,1)S(1)} %pad_maximum_fusion.3.tokens), channel_id=1, source_target_pairs={{0,1},{1,0},{2,3},{3,2},{4,5},{5,4},{6,7},{7,6},{8,9},{9,8},{10,11... | collective-permute-start | bytes 3145736 | tf_op jit(solution)/shard_map/ppermute | solution.py:21
  111.0 66.0 %collective-permute-start.15 = (bf16[64,2048]{1,0:T(8,128)(2,1)S(1)}, bf16[64,2048]{1,0:T(8,128)(2,1)S(1)}, u32[]{:S(2)}, u32[]{:S(2)}) collective-permute-start(bf16[64,2048]{1,0:T(8,128)(2,1)S(1)} %add_convert_fusion.16), channel_id=1, source_target_pairs={{0,4},{4,0},{8,12},{12,8},{16,20},{20,16},{24,28},{28,24},{1,5},{5... | collective-permute-start | bytes 786440 | tf_op jit(solution)/shard_map/ppermute | solution.py:21
  114.1 16.9 %collective-permute-start.34 = (bf16[128,2048]{1,0:T(8,128)(2,1)S(1)}, bf16[128,2048]{1,0:T(8,128)(2,1)S(1)}, u32[]{:S(2)}, u32[]{:S(2)}) collective-permute-start(bf16[128,2048]{1,0:T(8,128)(2,1)S(1)} %get-tuple-element.68), channel_id=1, source_target_pairs={{0,1},{1,0},{2,3},{3,2},{4,5},{5,4},{6,7},{7,6},{8,9},{9,8},{10,11... | collective-permute-start | bytes 1572872 | tf_op jit(solution)/shard_map/ppermute | solution.py:21
  132.6 14.1 %collective-permute-start.35 = (bf16[64,2048]{1,0:T(8,128)(2,1)S(1)}, bf16[64,2048]{1,0:T(8,128)(2,1)S(1)}, u32[]{:S(2)}, u32[]{:S(2)}) collective-permute-start(bf16[64,2048]{1,0:T(8,128)(2,1)S(1)} %add_convert_fusion.11), channel_id=1, source_target_pairs={{0,2},{1,3},{2,0},{3,1},{4,6},{5,7},{6,4},{7,5},{8,10},{9,11},{10,... | collective-permute-start | bytes 786440 | tf_op jit(solution)/shard_map/ppermute | solution.py:21
  134.2 12.3 %collective-permute-start.37 = (bf16[64,2048]{1,0:T(8,128)(2,1)S(1)}, bf16[64,2048]{1,0:T(8,128)(2,1)S(1)}, u32[]{:S(2)}, u32[]{:S(2)}) collective-permute-start(bf16[64,2048]{1,0:T(8,128)(2,1)S(1)} %add_convert_fusion.9), channel_id=1, source_target_pairs={{0,2},{1,3},{2,0},{3,1},{4,6},{5,7},{6,4},{7,5},{8,10},{9,11},{10,... | collective-permute-start | bytes 786440 | tf_op jit(solution)/shard_map/ppermute | solution.py:21
  146.5 13.1 %collective-permute-start.27 = (bf16[128,2048]{1,0:T(8,128)(2,1)S(1)}, bf16[128,2048]{1,0:T(8,128)(2,1)S(1)}, u32[]{:S(2)}, u32[]{:S(2)}) collective-permute-start(bf16[128,2048]{1,0:T(8,128)(2,1)S(1)} %add_convert_fusion.2), channel_id=1, source_target_pairs={{0,16},{4,20},{16,24},{20,28},{24,8},{28,12},{8,0},{12,4},{1,17},{... | collective-permute-start | bytes 1572872 | tf_op jit(solution)/shard_map/ppermute | solution.py:35
  147.1 14.1 %collective-permute-start.38 = (bf16[64,2048]{1,0:T(8,128)(2,1)S(1)}, bf16[64,2048]{1,0:T(8,128)(2,1)S(1)}, u32[]{:S(2)}, u32[]{:S(2)}) collective-permute-start(bf16[64,2048]{1,0:T(8,128)(2,1)S(1)} %add_convert_fusion.8), channel_id=1, source_target_pairs={{0,4},{4,0},{8,12},{12,8},{16,20},{20,16},{24,28},{28,24},{1,5},{5... | collective-permute-start | bytes 786440 | tf_op jit(solution)/shard_map/ppermute | solution.py:21
  148.6 18.9 %collective-permute-start.47 = (bf16[64,2048]{1,0:T(8,128)(2,1)S(1)}, bf16[64,2048]{1,0:T(8,128)(2,1)S(1)}, u32[]{:S(2)}, u32[]{:S(2)}) collective-permute-start(bf16[64,2048]{1,0:T(8,128)(2,1)S(1)} %add_convert_fusion.7), channel_id=1, source_target_pairs={{0,2},{1,3},{2,0},{3,1},{4,6},{5,7},{6,4},{7,5},{8,10},{9,11},{10,... | collective-permute-start | bytes 786440 | tf_op jit(solution)/shard_map/ppermute | solution.py:21
  161.7 12.0 %collective-permute-start.39 = (bf16[128,2048]{1,0:T(8,128)(2,1)S(1)}, bf16[128,2048]{1,0:T(8,128)(2,1)S(1)}, u32[]{:S(2)}, u32[]{:S(2)}) collective-permute-start(bf16[128,2048]{1,0:T(8,128)(2,1)S(1)} %add_convert_fusion.1), channel_id=1, source_target_pairs={{0,16},{4,20},{16,24},{20,28},{24,8},{28,12},{8,0},{12,4},{1,17},{... | collective-permute-start | bytes 1572872 | tf_op jit(solution)/shard_map/ppermute | solution.py:35
  174.1 12.4 %collective-permute-start.51 = (bf16[128,2048]{1,0:T(8,128)(2,1)S(1)}, bf16[128,2048]{1,0:T(8,128)(2,1)S(1)}, u32[]{:S(2)}, u32[]{:S(2)}) collective-permute-start(bf16[128,2048]{1,0:T(8,128)(2,1)S(1)} %add_convert_fusion), channel_id=1, source_target_pairs={{0,16},{4,20},{16,24},{20,28},{24,8},{28,12},{8,0},{12,4},{1,17},{... | collective-permute-start | bytes 1572872 | tf_op jit(solution)/shard_map/ppermute | solution.py:35
  (34 other events, 279.9 us)

commit v2 on v1

--- a/solution.py
+++ b/solution.py
@@ -95,11 +95,11 @@
     return sums
 
 
-def convolve_kernel(gated, kernel, gain, weight, out, total, squares, taps, gains, weights, extended, arrived, *, pad, rows):
+def convolve_kernel(gated, kernel, gain, out, total, squares, taps, gains, extended, arrived, *, pad, rows):
     length, channels = gated.shape
     moves = [
         pltpu.make_async_copy(source, target, arrived.at[i])
-        for i, (source, target) in enumerate(((kernel, taps), (gain, gains), (weight, weights)))
+        for i, (source, target) in enumerate(((kernel, taps), (gain, gains)))
     ]
     for move in moves:
         move.start()
@@ -124,7 +124,6 @@
 
     lax.fori_loop(0, length // rows, body, 0)
     moves[1].wait()
-    moves[2].wait()
 
 
 def head_kernel(before, gated, taps, total, squares, head, stats, extended):
@@ -156,7 +155,7 @@
     return tuple(pltpu.with_memory_space_constraint(a, pltpu.VMEM) for a in arrays)
 
 
-def convolve(glu_value, glu_gate, conv_kernel, norm_gain, mix_weight):
+def convolve(glu_value, glu_gate, conv_kernel, norm_gain):
     length, channels = glu_value.shape
     rows = min(128, length)
     pad = -(-(conv_kernel.shape[0] - 1) // 16) * 16
@@ -165,7 +164,7 @@
     gated = gated_rows(glu_value, glu_gate)
     norm_gain = norm_gain[None]
     vmem, hbm = pl.BlockSpec(memory_space=pltpu.VMEM), pl.BlockSpec(memory_space=pltpu.HBM)
-    convolved, total, squares, taps, gains, weights = pl.pallas_call(
+    convolved, total, squares, taps, gains = pl.pallas_call(
         lambda *refs: convolve_kernel(*refs, pad=pad, rows=rows),
         out_shape=(
             jax.ShapeDtypeStruct((length, channels), jnp.float32),
@@ -173,17 +172,16 @@
             pltpu.VMEM((length, 128), jnp.float32),
             pltpu.VMEM(conv_kernel.shape, jnp.float32),
             pltpu.VMEM(norm_gain.shape, jnp.float32),
-            pltpu.VMEM(mix_weight.shape, mix_weight.dtype),
         ),
-        in_specs=[vmem, hbm, hbm, hbm],
-        out_specs=(vmem,) * 6,
+        in_specs=[vmem, hbm, hbm],
+        out_specs=(vmem,) * 5,
         scratch_shapes=[
             pltpu.VMEM((length + pad + 8, channels), jnp.float32),
-            pltpu.SemaphoreType.DMA((3,)),
+            pltpu.SemaphoreType.DMA((2,)),
         ],
         compiler_params=pltpu.CompilerParams(vmem_limit_bytes=16 * 2**20),
         name="convolve",
-    )(*in_vmem(gated), *(pltpu.with_memory_space_constraint(a, pltpu.HBM) for a in (conv_kernel, norm_gain, mix_weight)))
+    )(*in_vmem(gated), *(pltpu.with_memory_space_constraint(a, pltpu.HBM) for a in (conv_kernel, norm_gain)))
     head, own = pl.pallas_call(
         head_kernel,
         out_shape=(pltpu.VMEM((pad, channels), jnp.float32), pltpu.VMEM((2, length), jnp.float32)),
@@ -194,11 +192,13 @@
         name="head",
     )(*in_vmem(before_rows, gated, taps, total, squares))
     stats = [own] + [swapped(own, "tp", d) for d in range(1, lax.axis_size("tp"))]
-    return convolved, head, stats, gains, weights
-
-
-def first_products_kernel(here, convolved, head, gain, mix_weight, *refs, bit, far, shares):
-    stats, (mix_in, send, keep, wide) = refs[:shares], refs[shares:]
+    return convolved, head, stats, gains
+
+
+def first_products_kernel(here, convolved, head, gain, weight, *refs, bit, far, shares):
+    stats, (mix_in, send, keep, wide, mix_weight, arrived) = refs[:shares], refs[shares:]
+    fetch = pltpu.make_async_copy(weight, mix_weight, arrived)
+    fetch.start()
     rows, channels = send.shape[0], convolved.shape[1] * shares
     sums = stats[0][...]
     for share in stats[1:]:
@@ -224,12 +224,16 @@
         values = jnp.concatenate([head[:, window], convolved[head.shape[0] :, window]], axis=0)
         normed = (values - centre) * scale * gain[:, window]
         mix_in[:, window] = (normed / (1.0 + jnp.exp(-normed))).astype(jnp.bfloat16)
+    fetch.wait()
     for d, out in ((far + bit, send), (far, keep)):
         own = mix_in[pl.ds(pl.multiple_of((here[0] ^ d) * rows, rows), rows), :]
         out[...] = matmul(own, mix_weight[...]).astype(out.dtype)
 
 
-def last_products_kernel(here, mix_in, mix_weight, send, keep, *, bit):
+def last_products_kernel(here, mix_in, weight, send, keep, mix_weight, arrived, *, bit):
+    fetch = pltpu.make_async_copy(weight, mix_weight, arrived)
+    fetch.start()
+    fetch.wait()
     rows = send.shape[0]
     for d, out in ((bit, send), (0, keep)):
         own = mix_in[pl.ds(pl.multiple_of((here[0] ^ d) * rows, rows), rows), :]
@@ -242,28 +246,32 @@
     rows, width = convolved.shape[0] // count, mix_weight.shape[1]
     here = lax.axis_index("tp").reshape(1).astype(jnp.int32)
     vmem, smem = pl.BlockSpec(memory_space=pltpu.VMEM), pl.BlockSpec(memory_space=pltpu.SMEM)
+    hbm = pl.BlockSpec(memory_space=pltpu.HBM)
+    mix_weight = pltpu.with_memory_space_constraint(mix_weight, pltpu.HBM)
+    fetched = [pltpu.VMEM(mix_weight.shape, mix_weight.dtype), pltpu.SemaphoreType.DMA]
     products = (pltpu.VMEM((rows, width), jnp.bfloat16), pltpu.VMEM((rows, width), jnp.float32))
     params = pltpu.CompilerParams(vmem_limit_bytes=8 * 2**20)
     mix_in, far_send, far_keep = pl.pallas_call(
         lambda *refs: first_products_kernel(*refs, bit=1, far=2, shares=count),
         out_shape=(pltpu.VMEM(convolved.shape, jnp.bfloat16),) + products,
-        in_specs=[smem] + [vmem] * (4 + count),
+        in_specs=[smem] + [vmem] * 3 + [hbm] + [vmem] * count,
         out_specs=(vmem,) * 3,
-        scratch_shapes=[pltpu.VMEM((8, convolved.shape[0]), jnp.float32)],
+        scratch_shapes=[pltpu.VMEM((8, convolved.shape[0]), jnp.float32)] + fetched,
         compiler_params=params,
         name="first_products",
-    )(here, convolved, *in_vmem(head, norm_gain, mix_weight, *stats))
+    )(here, *in_vmem(convolved, head, norm_gain), mix_weight, *in_vmem(*stats))
     arrived = swapped(far_send, "tp", 1)
     far_sum = (far_keep + arrived.astype(jnp.float32)).astype(jnp.bfloat16)
     from_chip = swapped(far_sum, "tp", 2)
     near_send, near_keep = pl.pallas_call(
         lambda *refs: last_products_kernel(*refs, bit=1),
         out_shape=products,
-        in_specs=[smem, vmem, vmem],
+        in_specs=[smem, vmem, hbm],
         out_specs=(vmem,) * 2,
+        scratch_shapes=fetched,
         compiler_params=params,
         name="last_products",
-    )(here, *in_vmem(mix_in, mix_weight))
+    )(here, *in_vmem(mix_in), mix_weight)
     arrived = swapped(near_send, "tp", 1)
     return near_keep, arrived, from_chip
 
@@ -271,6 +279,11 @@
 def hidden_kernel(residual, keep, from_core, from_chip, gain, out):
     values = residual[...].astype(jnp.float32) + keep[...]
     values = values + from_core[...].astype(jnp.float32) + from_chip[...].astype(jnp.float32)
+    out[...] = normalize(values, gain[...]).astype(out.dtype)
+
+
+def blended_kernel(hidden, own_share, carried, gain, out):
+    values = hidden[...].astype(jnp.float32) + (own_share[...] + carried[...].astype(jnp.float32))
     out[...] = normalize(values, gain[...]).astype(out.dtype)
 
 
@@ -288,7 +301,7 @@
     return onehot, jnp.sum(named * weights, axis=1)
 
 
-def routed_ring(hidden, ids, weights, gate_local, up_local, down_local, capacity):
+def routed_ring(hidden, ids, weights, gate_local, up_local, down_local, out_gain, capacity):
     steps = lax.axis_size("sp") // 2
     here = lax.axis_index("sp").astype(jnp.float32)
     other = (lax.axis_index("sp") ^ 1).astype(jnp.float32)
@@ -335,7 +348,15 @@
         if s:
             carried = around(share, 1)
         block = following
-    return own_share + carried.astype(jnp.float32)
+    vmem = pl.BlockSpec(memory_space=pltpu.VMEM)
+    return pl.pallas_call(
+        blended_kernel,
+        out_shape=jax.ShapeDtypeStruct(hidden.shape, jnp.bfloat16),
+        in_specs=[vmem] * 4,
+        out_specs=vmem,
+        compiler_params=pltpu.CompilerParams(vmem_limit_bytes=8 * 2**20),
+        name="blended",
+    )(*in_vmem(hidden, own_share, carried, out_gain[None]))
 
 
 def slot_layout(route_ids, experts, capacity):
@@ -350,7 +371,7 @@
     return (slot_table, position.reshape(row_count, top_count))
 
 
-def routed_exchange(hidden, ids, weights, gate_local, up_local, down_local, capacity):
+def routed_exchange(hidden, ids, weights, gate_local, up_local, down_local, out_gain, capacity):
     experts = lax.axis_size("sp")
     own_count, width = hidden.shape
     top_count = ids.shape[1]
@@ -367,7 +388,8 @@
     returned = lax.all_to_all(expert_out, "sp", split_axis=0, concat_axis=0, tiled=True)
     picked = returned.reshape(experts * capacity, width)[positions.reshape(-1)]
     picked = picked.reshape(own_count, top_count, width)
-    return jnp.einsum("tk,tkd->td", weights, picked.astype(jnp.float32))
+    routed_sum = jnp.einsum("tk,tkd->td", weights, picked.astype(jnp.float32))
+    return normalize(hidden.astype(jnp.float32) + routed_sum, out_gain).astype(jnp.bfloat16)
 
 
 def shards(
@@ -385,8 +407,8 @@
     w_down,
     out_gain,
 ):
-    convolved, head, stats, gains, weights = convolve(glu_value, glu_gate, conv_kernel, norm_gain, mix_weight)
-    mixed_rows = scattered_product(convolved, head, stats, gains, weights)
+    convolved, head, stats, gains = convolve(glu_value, glu_gate, conv_kernel, norm_gain)
+    mixed_rows = scattered_product(convolved, head, stats, gains, mix_weight)
     vmem = pl.BlockSpec(memory_space=pltpu.VMEM)
     hidden = pl.pallas_call(
         hidden_kernel,
@@ -403,8 +425,7 @@
     padded_rows = (experts - 1) * capacity
     ring = lax.axis_size("tp") == 4 and whole_rows <= 2 * padded_rows
     route = routed_ring if ring else routed_exchange
-    routed_sum = route(hidden, expert_ids, route_weight, w_gate[0], w_up[0], w_down[0], capacity)
-    return normalize(hidden.astype(jnp.float32) + routed_sum, out_gain).astype(jnp.bfloat16)
+    return route(hidden, expert_ids, route_weight, w_gate[0], w_up[0], w_down[0], out_gain, capacity)
 
 
 def solution(mesh):

time: 189 us -> 194 us (1.026)
  waiting for transfers between devices: 100 us -> 114 us
  starting transfers between devices: 50.6 us -> 40.2 us
  Pallas kernels: 22.7 us -> 26.3 us
    ppermute x42, waiting for transfers between devices: 76.9 us -> 90.1 us  [swapped(): lax.ppermute(block, axis, [(i, i ^ bit) for i in range(lax.axis_size(axis...]
    ppermute x42, starting transfers between devices: 31.4 us -> 24.9 us  [swapped(): lax.ppermute(block, axis, [(i, i ^ bit) for i in range(lax.axis_size(axis...]
    ppermute x9, starting transfers between devices: 15.8 us -> 11.9 us  [around(): return lax.ppermute(block, 'sp', route)]
  transfers between devices with their start and end apart: 52 -> 52, of which waited for: 27 -> 27; matrix products, arithmetic and copies ran while one was open for 6% -> 6% of each run, Pallas kernels for 12% -> 13%
where the time goes in v2:
time: 194 us; the launch traced here: 193 us
  waiting for transfers between devices  114 us (59%)
  starting transfers between devices  40.2 us (21%)
  Pallas kernels  26.3 us (14%)
  other arithmetic  6.57 us (3%)
  matrix products  5.61 us (3%)
    ppermute x42, waiting for transfers between devices, swapped(): lax.ppermute(block, axis, [(i, i ^ bit) for i in range(lax.axis_size(axis...  90.1 us
    ppermute x42, starting transfers between devices, swapped(): lax.ppermute(block, axis, [(i, i ^ bit) for i in range(lax.axis_size(axis...  24.9 us
    ppermute x9, waiting for transfers between devices, around(): return lax.ppermute(block, 'sp', route)  23.7 us
    pallas_call x8, Pallas kernels, expert_step(): pl.pallas_call(expert_kernel, out_shape=(jax.ShapeDtypeStruct((rows // pa...  15.2 us
    ppermute x9, starting transfers between devices, around(): return lax.ppermute(block, 'sp', route)  11.9 us
    dot_general x16, matrix products, matmul(): return jnp.dot(a, b, preferred_element_type=jnp.float32)  5.61 us
  transfers between devices with their start and end apart: 52, of which 27 were waited for; matrix products, arithmetic and copies ran while one was open for 6% of the time, Pallas kernels for 13%

profile of v2, /device:TPU:0, one launch (start us, length us, event | category | flops | bytes accessed | tf_op | source)
XLA Modules:
  0.0 193.2 jit_solution(14539460353468042123)
XLA Ops:
  1.4 3.1 %collective-permute-start.40 = (f32[128,4]{0,1:T(4,128)S(1)}, f32[128,4]{0,1:T(4,128)S(1)}, u32[]{:S(2)}, u32[]{:S(2)}) collective-permute-start(f32[128,4]{0,1:T(4,128)S(1)} %pad_maximum_fusion.4), channel_id=1, source_target_pairs={{0,8},{4,12},{16,0},{20,4},{24,16},{28,20},{8,24},{12,28},{1,9},{5... | collective-permute-start | bytes 6152 | tf_op jit(solution)/shard_map/ppermute | solution.py:35
  4.4 2.5 %collective-permute-start.28 = (f32[128,4]{0,1:T(4,128)S(1)}, f32[128,4]{0,1:T(4,128)S(1)}, u32[]{:S(2)}, u32[]{:S(2)}) collective-permute-start(f32[128,4]{0,1:T(4,128)S(1)} %pad_maximum_fusion.4), channel_id=1, source_target_pairs={{0,24},{4,28},{16,8},{20,12},{24,0},{28,4},{8,16},{12,20},{1,25},{... | collective-permute-start | bytes 6152 | tf_op jit(solution)/shard_map/ppermute | solution.py:35
  9.3 3.4 %collective-permute-start = (bf16[32,512]{1,0:T(8,128)(2,1)S(1)}, bf16[32,512]{1,0:T(8,128)(2,1)S(1)}, u32[]{:S(2)}, u32[]{:S(2)}) collective-permute-start(bf16[32,512]{1,0:T(8,128)(2,1)S(1)} %multiply_convert_fusion.1), channel_id=1, source_target_pairs={{0,4},{4,8},{8,12},{12,16},{16,20},{20,24},{24,28},{1,5},{5,9},{9,... | collective-permute-start | bytes 98312 | tf_op jit(solution)/shard_map/ppermute | solution.py:17
  15.2 3.8 %convolve.1 = (f32[512,512]{1,0:T(8,128)S(1)}, f32[512,128]{1,0:T(8,128)S(1)}, f32[512,128]{1,0:T(8,128)S(1)}, f32[31,512]{1,0:T(8,128)S(1)}, f32[1,512]{1,0:T(1,128)S(1)}) custom-call(bf16[512,512]{1,0:T(8,128)(2,1)S(1)} %multiply_convert_fusion.refs_0_.gated, f32[31,512]{1,0:T(8,128)} %refs_1_.1, f32[1,512]{1,0:T(1,128)} %bitcast.45), custom_call_target="tpu_custom_call" | custom-call | tf_op jit(solution)/shard_map/convolve/pallas_call | solution.py:167
  24.7 2.4 %first_products.1 = (bf16[512,512]{1,0:T(8,128)(2,1)S(1)}, bf16[128,2048]{1,0:T(8,128)(2,1)S(1)}, f32[128,2048]{1,0:T(8,128)S(1)}) custom-call(s32[1]{0:T(128)} %bitcast.refs_0_, f32[512,512]{1,0:T(8,128)S(1)} %get-tuple-element.41.refs_1_, f32[32,512]{1,0:T(8,128)S(1)} %get-tuple-element.45.refs_2_, f32[1,512]{1,0:T(1,128)S(1)} %get-tuple-element.46.refs_3_, ...), custom_call_target="tpu_custom_call" | custom-call | tf_op jit(solution)/shard_map/first_products/pallas_call | solution.py:254
  27.4 2.5 %last_products.1 = (bf16[128,2048]{1,0:T(8,128)(2,1)S(1)}, f32[128,2048]{1,0:T(8,128)S(1)}) custom-call(s32[1]{0:T(128)} %bitcast.refs_0_, bf16[512,512]{1,0:T(8,128)(2,1)S(1)} %get-tuple-element.48.refs_1_, bf16[512,2048]{1,0:T(8,128)(2,1)} %refs_2_.1), custom_call_target="tpu_custom_call" | custom-call | tf_op jit(solution)/shard_map/last_products/pallas_call | solution.py:266
  31.9 12.6 %collective-permute-done.6.from_chip = bf16[128,2048]{1,0:T(8,128)(2,1)S(1)} collective-permute-done((bf16[128,2048]{1,0:T(8,128)(2,1)S(1)}, bf16[128,2048]{1,0:T(8,128)(2,1)S(1)}, u32[]{:S(2)}, u32[]{:S(2)}) %collective-permute-start.6) | collective-permute-done | bytes 524320 | tf_op jit(solution)/shard_map/ppermute | solution.py:21
  48.0 5.1 %collective-permute-done.7 = bf16[64,2048]{1,0:T(8,128)(2,1)S(1)} collective-permute-done((bf16[64,2048]{1,0:T(8,128)(2,1)S(1)}, bf16[64,2048]{1,0:T(8,128)(2,1)S(1)}, u32[]{:S(2)}, u32[]{:S(2)}) %collective-permute-start.7) | collective-permute-done | bytes 262176 | tf_op jit(solution)/shard_map/ppermute | solution.py:21
  53.6 4.7 %collective-permute-done.17 = bf16[128,2048]{1,0:T(8,128)(2,1)S(1)} collective-permute-done((bf16[128,2048]{1,0:T(8,128)(2,1)S(1)}, bf16[128,2048]{1,0:T(8,128)(2,1)S(1)}, u32[]{:S(2)}, u32[]{:S(2)}) %collective-permute-start.17) | collective-permute-done | bytes 524320 | tf_op jit(solution)/shard_map/ppermute | solution.py:35
  62.1 3.3 %collective-permute-done.18 = bf16[64,2048]{1,0:T(8,128)(2,1)S(1)} collective-permute-done((bf16[64,2048]{1,0:T(8,128)(2,1)S(1)}, bf16[64,2048]{1,0:T(8,128)(2,1)S(1)}, u32[]{:S(2)}, u32[]{:S(2)}) %collective-permute-start.18) | collective-permute-done | bytes 262176 | tf_op jit(solution)/shard_map/ppermute | solution.py:21
  67.8 3.3 %collective-permute-done.29 = bf16[128,2048]{1,0:T(8,128)(2,1)S(1)} collective-permute-done((bf16[128,2048]{1,0:T(8,128)(2,1)S(1)}, bf16[128,2048]{1,0:T(8,128)(2,1)S(1)}, u32[]{:S(2)}, u32[]{:S(2)}) %collective-permute-start.29) | collective-permute-done | bytes 524320 | tf_op jit(solution)/shard_map/ppermute | solution.py:35
  80.3 4.3 %collective-permute-done.41 = bf16[128,2048]{1,0:T(8,128)(2,1)S(1)} collective-permute-done((bf16[128,2048]{1,0:T(8,128)(2,1)S(1)}, bf16[128,2048]{1,0:T(8,128)(2,1)S(1)}, u32[]{:S(2)}, u32[]{:S(2)}) %collective-permute-start.41) | collective-permute-done | bytes 524320 | tf_op jit(solution)/shard_map/ppermute | solution.py:35
  85.6 4.6 %collective-permute-done.31 = bf16[64,2048]{1,0:T(8,128)(2,1)S(1)} collective-permute-done((bf16[64,2048]{1,0:T(8,128)(2,1)S(1)}, bf16[64,2048]{1,0:T(8,128)(2,1)S(1)}, u32[]{:S(2)}, u32[]{:S(2)}) %collective-permute-start.31) | collective-permute-done | bytes 262176 | tf_op jit(solution)/shard_map/ppermute | solution.py:21
  96.7 3.2 %collective-permute-done.44 = bf16[64,2048]{1,0:T(8,128)(2,1)S(1)} collective-permute-done((bf16[64,2048]{1,0:T(8,128)(2,1)S(1)}, bf16[64,2048]{1,0:T(8,128)(2,1)S(1)}, u32[]{:S(2)}, u32[]{:S(2)}) %collective-permute-start.44) | collective-permute-done | bytes 262176 | tf_op jit(solution)/shard_map/ppermute | solution.py:21
  99.9 5.1 %collective-permute-done.43 = bf16[64,2048]{1,0:T(8,128)(2,1)S(1)} collective-permute-done((bf16[64,2048]{1,0:T(8,128)(2,1)S(1)}, bf16[64,2048]{1,0:T(8,128)(2,1)S(1)}, u32[]{:S(2)}, u32[]{:S(2)}) %collective-permute-start.43) | collective-permute-done | bytes 262176 | tf_op jit(solution)/shard_map/ppermute | solution.py:21
  110.4 8.1 %collective-permute-done.14 = bf16[64,2048]{1,0:T(8,128)(2,1)S(1)} collective-permute-done((bf16[64,2048]{1,0:T(8,128)(2,1)S(1)}, bf16[64,2048]{1,0:T(8,128)(2,1)S(1)}, u32[]{:S(2)}, u32[]{:S(2)}) %collective-permute-start.14) | collective-permute-done | bytes 262176 | tf_op jit(solution)/shard_map/ppermute | solution.py:21
  124.0 7.9 %collective-permute-done.25 = bf16[64,2048]{1,0:T(8,128)(2,1)S(1)} collective-permute-done((bf16[64,2048]{1,0:T(8,128)(2,1)S(1)}, bf16[64,2048]{1,0:T(8,128)(2,1)S(1)}, u32[]{:S(2)}, u32[]{:S(2)}) %collective-permute-start.25) | collective-permute-done | bytes 262176 | tf_op jit(solution)/shard_map/ppermute | solution.py:21
  132.7 6.7 %collective-permute-done.23 = bf16[64,2048]{1,0:T(8,128)(2,1)S(1)} collective-permute-done((bf16[64,2048]{1,0:T(8,128)(2,1)S(1)}, bf16[64,2048]{1,0:T(8,128)(2,1)S(1)}, u32[]{:S(2)}, u32[]{:S(2)}) %collective-permute-start.23) | collective-permute-done | bytes 262176 | tf_op jit(solution)/shard_map/ppermute | solution.py:21
  145.3 3.2 %collective-permute-done.26 = bf16[64,2048]{1,0:T(8,128)(2,1)S(1)} collective-permute-done((bf16[64,2048]{1,0:T(8,128)(2,1)S(1)}, bf16[64,2048]{1,0:T(8,128)(2,1)S(1)}, u32[]{:S(2)}, u32[]{:S(2)}) %collective-permute-start.26) | collective-permute-done | bytes 262176 | tf_op jit(solution)/shard_map/ppermute | solution.py:21
  150.5 4.7 %collective-permute-done.35 = bf16[64,2048]{1,0:T(8,128)(2,1)S(1)} collective-permute-done((bf16[64,2048]{1,0:T(8,128)(2,1)S(1)}, bf16[64,2048]{1,0:T(8,128)(2,1)S(1)}, u32[]{:S(2)}, u32[]{:S(2)}) %collective-permute-start.35) | collective-permute-done | bytes 262176 | tf_op jit(solution)/shard_map/ppermute | solution.py:21
  156.7 7.7 %collective-permute-done.38 = bf16[64,2048]{1,0:T(8,128)(2,1)S(1)} collective-permute-done((bf16[64,2048]{1,0:T(8,128)(2,1)S(1)}, bf16[64,2048]{1,0:T(8,128)(2,1)S(1)}, u32[]{:S(2)}, u32[]{:S(2)}) %collective-permute-start.38) | collective-permute-done | bytes 262176 | tf_op jit(solution)/shard_map/ppermute | solution.py:21
  167.0 6.5 %collective-permute-done.49 = bf16[64,2048]{1,0:T(8,128)(2,1)S(1)} collective-permute-done((bf16[64,2048]{1,0:T(8,128)(2,1)S(1)}, bf16[64,2048]{1,0:T(8,128)(2,1)S(1)}, u32[]{:S(2)}, u32[]{:S(2)}) %collective-permute-start.49) | collective-permute-done | bytes 262176 | tf_op jit(solution)/shard_map/ppermute | solution.py:21
  174.7 3.1 %collective-permute-done.47 = bf16[64,2048]{1,0:T(8,128)(2,1)S(1)} collective-permute-done((bf16[64,2048]{1,0:T(8,128)(2,1)S(1)}, bf16[64,2048]{1,0:T(8,128)(2,1)S(1)}, u32[]{:S(2)}, u32[]{:S(2)}) %collective-permute-start.47) | collective-permute-done | bytes 262176 | tf_op jit(solution)/shard_map/ppermute | solution.py:21
  181.5 10.4 %collective-permute-done.51.carried = bf16[128,2048]{1,0:T(8,128)(2,1)S(1)} collective-permute-done((bf16[128,2048]{1,0:T(8,128)(2,1)S(1)}, bf16[128,2048]{1,0:T(8,128)(2,1)S(1)}, u32[]{:S(2)}, u32[]{:S(2)}) %collective-permute-start.51) | collective-permute-done | bytes 524320 | tf_op jit(solution)/shard_map/ppermute | solution.py:35
  (164 shorter events, 70.2 us)
Async XLA Ops:
  1.4 17.6 %collective-permute-start.40 = (f32[128,4]{0,1:T(4,128)S(1)}, f32[128,4]{0,1:T(4,128)S(1)}, u32[]{:S(2)}, u32[]{:S(2)}) collective-permute-start(f32[128,4]{0,1:T(4,128)S(1)} %pad_maximum_fusion.4), channel_id=1, source_target_pairs={{0,8},{4,12},{16,0},{20,4},{24,16},{28,20},{8,24},{12,28},{1,9},{5... | collective-permute-start | bytes 6152 | tf_op jit(solution)/shard_map/ppermute | solution.py:35
  4.4 14.8 %collective-permute-start.28 = (f32[128,4]{0,1:T(4,128)S(1)}, f32[128,4]{0,1:T(4,128)S(1)}, u32[]{:S(2)}, u32[]{:S(2)}) collective-permute-start(f32[128,4]{0,1:T(4,128)S(1)} %pad_maximum_fusion.4), channel_id=1, source_target_pairs={{0,24},{4,28},{16,8},{20,12},{24,0},{28,4},{8,16},{12,20},{1,25},{... | collective-permute-start | bytes 6152 | tf_op jit(solution)/shard_map/ppermute | solution.py:35
  6.9 20.5 %collective-permute-start.16 = (f32[128,4]{0,1:T(4,128)S(1)}, f32[128,4]{0,1:T(4,128)S(1)}, u32[]{:S(2)}, u32[]{:S(2)}) collective-permute-start(f32[128,4]{0,1:T(4,128)S(1)} %pad_maximum_fusion.4), channel_id=1, source_target_pairs={{0,16},{4,20},{16,24},{20,28},{24,8},{28,12},{8,0},{12,4},{1,17},{... | collective-permute-start | bytes 6152 | tf_op jit(solution)/shard_map/ppermute | solution.py:35
  30.4 14.1 %collective-permute-start.6 = (bf16[128,2048]{1,0:T(8,128)(2,1)S(1)}, bf16[128,2048]{1,0:T(8,128)(2,1)S(1)}, u32[]{:S(2)}, u32[]{:S(2)}) collective-permute-start(bf16[128,2048]{1,0:T(8,128)(2,1)S(1)} %add_convert_fusion.3), channel_id=1, source_target_pairs={{0,2},{1,3},{2,0},{3,1},{4,6},{5,7},{6,4},{7,5},{8,10},{9,11},{10,... | collective-permute-start | bytes 1572872 | tf_op jit(solution)/shard_map/ppermute | solution.py:21
  45.0 13.2 %collective-permute-start.17 = (bf16[128,2048]{1,0:T(8,128)(2,1)S(1)}, bf16[128,2048]{1,0:T(8,128)(2,1)S(1)}, u32[]{:S(2)}, u32[]{:S(2)}) collective-permute-start(bf16[128,2048]{1,0:T(8,128)(2,1)S(1)} %hidden.1), channel_id=1, source_target_pairs={{0,16},{4,20},{16,24},{20,28},{24,8},{28,12},{8,0},{12,4},{1,17},{... | collective-permute-start | bytes 1572872 | tf_op jit(solution)/shard_map/ppermute | solution.py:35
  47.4 14.5 %collective-permute-start.9 = (bf16[64,2048]{1,0:T(8,128)(2,1)S(1)}, bf16[64,2048]{1,0:T(8,128)(2,1)S(1)}, u32[]{:S(2)}, u32[]{:S(2)}) collective-permute-start(bf16[64,2048]{1,0:T(8,128)(2,1)S(1)} %convolution_convert_fusion.6), channel_id=1, source_target_pairs={{0,2},{1,3},{2,0},{3,1},{4,6},{5,7},{6,4},{7,5},{8,10},{9,11},{10,... | collective-permute-start | bytes 786440 | tf_op jit(solution)/shard_map/ppermute | solution.py:21
  59.1 12.0 %collective-permute-start.29 = (bf16[128,2048]{1,0:T(8,128)(2,1)S(1)}, bf16[128,2048]{1,0:T(8,128)(2,1)S(1)}, u32[]{:S(2)}, u32[]{:S(2)}) collective-permute-start(bf16[128,2048]{1,0:T(8,128)(2,1)S(1)} %collective-permute-done.17), channel_id=1, source_target_pairs={{0,16},{4,20},{16,24},{20,28},{24,8},{28,12},{8,0},{12,4},{1,17},{... | collective-permute-start | bytes 1572872 | tf_op jit(solution)/shard_map/ppermute | solution.py:35
  61.3 14.0 %collective-permute-start.20 = (bf16[64,2048]{1,0:T(8,128)(2,1)S(1)}, bf16[64,2048]{1,0:T(8,128)(2,1)S(1)}, u32[]{:S(2)}, u32[]{:S(2)}) collective-permute-start(bf16[64,2048]{1,0:T(8,128)(2,1)S(1)} %convolution_convert_fusion.4), channel_id=1, source_target_pairs={{0,2},{1,3},{2,0},{3,1},{4,6},{5,7},{6,4},{7,5},{8,10},{9,11},{10,... | collective-permute-start | bytes 786440 | tf_op jit(solution)/shard_map/ppermute | solution.py:21
  62.0 32.7 %collective-permute-start.10 = (bf16[256,2048]{1,0:T(8,128)(2,1)S(1)}, bf16[256,2048]{1,0:T(8,128)(2,1)S(1)}, u32[]{:S(2)}, u32[]{:S(2)}) collective-permute-start(bf16[256,2048]{1,0:T(8,128)(2,1)S(1)} %pad_maximum_fusion.tokens), channel_id=1, source_target_pairs={{0,1},{1,0},{2,3},{3,2},{4,5},{5,4},{6,7},{7,6},{8,9},{9,8},{10,11... | collective-permute-start | bytes 3145736 | tf_op jit(solution)/shard_map/ppermute | solution.py:21
  75.4 31.8 %collective-permute-start.21 = (bf16[256,2048]{1,0:T(8,128)(2,1)S(1)}, bf16[256,2048]{1,0:T(8,128)(2,1)S(1)}, u32[]{:S(2)}, u32[]{:S(2)}) collective-permute-start(bf16[256,2048]{1,0:T(8,128)(2,1)S(1)} %pad_maximum_fusion.1.tokens), channel_id=1, source_target_pairs={{0,1},{1,0},{2,3},{3,2},{4,5},{5,4},{6,7},{7,6},{8,9},{9,8},{10,11... | collective-permute-start | bytes 3145736 | tf_op jit(solution)/shard_map/ppermute | solution.py:21
  77.9 12.3 %collective-permute-start.31 = (bf16[64,2048]{1,0:T(8,128)(2,1)S(1)}, bf16[64,2048]{1,0:T(8,128)(2,1)S(1)}, u32[]{:S(2)}, u32[]{:S(2)}) collective-permute-start(bf16[64,2048]{1,0:T(8,128)(2,1)S(1)} %collective-permute-done.30), channel_id=1, source_target_pairs={{0,2},{1,3},{2,0},{3,1},{4,6},{5,7},{6,4},{7,5},{8,10},{9,11},{10,... | collective-permute-start | bytes 786440 | tf_op jit(solution)/shard_map/ppermute | solution.py:21
  90.3 28.8 %collective-permute-start.33 = (bf16[256,2048]{1,0:T(8,128)(2,1)S(1)}, bf16[256,2048]{1,0:T(8,128)(2,1)S(1)}, u32[]{:S(2)}, u32[]{:S(2)}) collective-permute-start(bf16[256,2048]{1,0:T(8,128)(2,1)S(1)} %pad_maximum_fusion.2.tokens), channel_id=1, source_target_pairs={{0,1},{1,0},{2,3},{3,2},{4,5},{5,4},{6,7},{7,6},{8,9},{9,8},{10,11... | collective-permute-start | bytes 3145736 | tf_op jit(solution)/shard_map/ppermute | solution.py:21
  91.4 13.7 %collective-permute-start.43 = (bf16[64,2048]{1,0:T(8,128)(2,1)S(1)}, bf16[64,2048]{1,0:T(8,128)(2,1)S(1)}, u32[]{:S(2)}, u32[]{:S(2)}) collective-permute-start(bf16[64,2048]{1,0:T(8,128)(2,1)S(1)} %collective-permute-done.42), channel_id=1, source_target_pairs={{0,2},{1,3},{2,0},{3,1},{4,6},{5,7},{6,4},{7,5},{8,10},{9,11},{10,... | collective-permute-start | bytes 786440 | tf_op jit(solution)/shard_map/ppermute | solution.py:21
  96.6 13.2 %collective-permute-start.11 = (bf16[128,2048]{1,0:T(8,128)(2,1)S(1)}, bf16[128,2048]{1,0:T(8,128)(2,1)S(1)}, u32[]{:S(2)}, u32[]{:S(2)}) collective-permute-start(bf16[128,2048]{1,0:T(8,128)(2,1)S(1)} %get-tuple-element.54), channel_id=1, source_target_pairs={{0,1},{1,0},{2,3},{3,2},{4,5},{5,4},{6,7},{7,6},{8,9},{9,8},{10,11... | collective-permute-start | bytes 1572872 | tf_op jit(solution)/shard_map/ppermute | solution.py:21
  105.2 37.2 %collective-permute-start.45 = (bf16[256,2048]{1,0:T(8,128)(2,1)S(1)}, bf16[256,2048]{1,0:T(8,128)(2,1)S(1)}, u32[]{:S(2)}, u32[]{:S(2)}) collective-permute-start(bf16[256,2048]{1,0:T(8,128)(2,1)S(1)} %pad_maximum_fusion.3.tokens), channel_id=1, source_target_pairs={{0,1},{1,0},{2,3},{3,2},{4,5},{5,4},{6,7},{7,6},{8,9},{9,8},{10,11... | collective-permute-start | bytes 3145736 | tf_op jit(solution)/shard_map/ppermute | solution.py:21
  109.1 13.0 %collective-permute-start.24 = (bf16[128,2048]{1,0:T(8,128)(2,1)S(1)}, bf16[128,2048]{1,0:T(8,128)(2,1)S(1)}, u32[]{:S(2)}, u32[]{:S(2)}) collective-permute-start(bf16[128,2048]{1,0:T(8,128)(2,1)S(1)} %get-tuple-element.63), channel_id=1, source_target_pairs={{0,1},{1,0},{2,3},{3,2},{4,5},{5,4},{6,7},{7,6},{8,9},{9,8},{10,11... | collective-permute-start | bytes 1572872 | tf_op jit(solution)/shard_map/ppermute | solution.py:21
  109.7 12.6 %collective-permute-start.22 = (bf16[128,2048]{1,0:T(8,128)(2,1)S(1)}, bf16[128,2048]{1,0:T(8,128)(2,1)S(1)}, u32[]{:S(2)}, u32[]{:S(2)}) collective-permute-start(bf16[128,2048]{1,0:T(8,128)(2,1)S(1)} %get-tuple-element.60), channel_id=1, source_target_pairs={{0,1},{1,0},{2,3},{3,2},{4,5},{5,4},{6,7},{7,6},{8,9},{9,8},{10,11... | collective-permute-start | bytes 1572872 | tf_op jit(solution)/shard_map/ppermute | solution.py:21
  118.5 62.6 %collective-permute-start.12 = (bf16[64,2048]{1,0:T(8,128)(2,1)S(1)}, bf16[64,2048]{1,0:T(8,128)(2,1)S(1)}, u32[]{:S(2)}, u32[]{:S(2)}) collective-permute-start(bf16[64,2048]{1,0:T(8,128)(2,1)S(1)} %add_convert_fusion.19), channel_id=1, source_target_pairs={{0,2},{1,3},{2,0},{3,1},{4,6},{5,7},{6,4},{7,5},{8,10},{9,11},{10,... | collective-permute-start | bytes 786440 | tf_op jit(solution)/shard_map/ppermute | solution.py:21
  119.1 61.7 %collective-permute-start.15 = (bf16[64,2048]{1,0:T(8,128)(2,1)S(1)}, bf16[64,2048]{1,0:T(8,128)(2,1)S(1)}, u32[]{:S(2)}, u32[]{:S(2)}) collective-permute-start(bf16[64,2048]{1,0:T(8,128)(2,1)S(1)} %add_convert_fusion.16), channel_id=1, source_target_pairs={{0,4},{4,0},{8,12},{12,8},{16,20},{20,16},{24,28},{28,24},{1,5},{5... | collective-permute-start | bytes 786440 | tf_op jit(solution)/shard_map/ppermute | solution.py:21
  122.1 17.6 %collective-permute-start.36 = (bf16[128,2048]{1,0:T(8,128)(2,1)S(1)}, bf16[128,2048]{1,0:T(8,128)(2,1)S(1)}, u32[]{:S(2)}, u32[]{:S(2)}) collective-permute-start(bf16[128,2048]{1,0:T(8,128)(2,1)S(1)} %get-tuple-element.69), channel_id=1, source_target_pairs={{0,1},{1,0},{2,3},{3,2},{4,5},{5,4},{6,7},{7,6},{8,9},{9,8},{10,11... | collective-permute-start | bytes 1572872 | tf_op jit(solution)/shard_map/ppermute | solution.py:21
  142.4 12.8 %collective-permute-start.35 = (bf16[64,2048]{1,0:T(8,128)(2,1)S(1)}, bf16[64,2048]{1,0:T(8,128)(2,1)S(1)}, u32[]{:S(2)}, u32[]{:S(2)}) collective-permute-start(bf16[64,2048]{1,0:T(8,128)(2,1)S(1)} %add_convert_fusion.11), channel_id=1, source_target_pairs={{0,2},{1,3},{2,0},{3,1},{4,6},{5,7},{6,4},{7,5},{8,10},{9,11},{10,... | collective-permute-start | bytes 786440 | tf_op jit(solution)/shard_map/ppermute | solution.py:21
  150.4 15.0 %collective-permute-start.27 = (bf16[128,2048]{1,0:T(8,128)(2,1)S(1)}, bf16[128,2048]{1,0:T(8,128)(2,1)S(1)}, u32[]{:S(2)}, u32[]{:S(2)}) collective-permute-start(bf16[128,2048]{1,0:T(8,128)(2,1)S(1)} %add_convert_fusion.2), channel_id=1, source_target_pairs={{0,16},{4,20},{16,24},{20,28},{24,8},{28,12},{8,0},{12,4},{1,17},{... | collective-permute-start | bytes 1572872 | tf_op jit(solution)/shard_map/ppermute | solution.py:35
  165.9 13.2 %collective-permute-start.39 = (bf16[128,2048]{1,0:T(8,128)(2,1)S(1)}, bf16[128,2048]{1,0:T(8,128)(2,1)S(1)}, u32[]{:S(2)}, u32[]{:S(2)}) collective-permute-start(bf16[128,2048]{1,0:T(8,128)(2,1)S(1)} %add_convert_fusion.1), channel_id=1, source_target_pairs={{0,16},{4,20},{16,24},{20,28},{24,8},{28,12},{8,0},{12,4},{1,17},{... | collective-permute-start | bytes 1572872 | tf_op jit(solution)/shard_map/ppermute | solution.py:35
  166.0 11.8 %collective-permute-start.47 = (bf16[64,2048]{1,0:T(8,128)(2,1)S(1)}, bf16[64,2048]{1,0:T(8,128)(2,1)S(1)}, u32[]{:S(2)}, u32[]{:S(2)}) collective-permute-start(bf16[64,2048]{1,0:T(8,128)(2,1)S(1)} %add_convert_fusion.7), channel_id=1, source_target_pairs={{0,2},{1,3},{2,0},{3,1},{4,6},{5,7},{6,4},{7,5},{8,10},{9,11},{10,... | collective-permute-start | bytes 786440 | tf_op jit(solution)/shard_map/ppermute | solution.py:21
  (34 other events, 313.5 us)

commit v3 on v2

--- a/solution.py
+++ b/solution.py
@@ -73,7 +73,7 @@
         cost_estimate=pl.CostEstimate(
             flops=6 * rows * width * gate_matrix.shape[1], transcendentals=0, bytes_accessed=0
         ),
-        name="expert_step",
+        name="expert",
     )(tokens, gate_matrix, up_matrix, down_matrix)
 
 
@@ -258,7 +258,7 @@
         out_specs=(vmem,) * 3,
         scratch_shapes=[pltpu.VMEM((8, convolved.shape[0]), jnp.float32)] + fetched,
         compiler_params=params,
-        name="first_products",
+        name="fp",
     )(here, *in_vmem(convolved, head, norm_gain), mix_weight, *in_vmem(*stats))
     arrived = swapped(far_send, "tp", 1)
     far_sum = (far_keep + arrived.astype(jnp.float32)).astype(jnp.bfloat16)
@@ -270,7 +270,7 @@
         out_specs=(vmem,) * 2,
         scratch_shapes=fetched,
         compiler_params=params,
-        name="last_products",
+        name="lp",
     )(here, *in_vmem(mix_in), mix_weight)
     arrived = swapped(near_send, "tp", 1)
     return near_keep, arrived, from_chip

time: 194 us -> 194 us (level)
  no operation moved by 1% of the time
where the time goes in v3:
time: 194 us; the launch traced here: 193 us
  waiting for transfers between devices  114 us (59%)
  starting transfers between devices  40.2 us (21%)
  Pallas kernels  26.3 us (14%)
  other arithmetic  6.57 us (3%)
  matrix products  5.61 us (3%)
    ppermute x42, waiting for transfers between devices, swapped(): lax.ppermute(block, axis, [(i, i ^ bit) for i in range(lax.axis_size(axis...  90.1 us
    ppermute x42, starting transfers between devices, swapped(): lax.ppermute(block, axis, [(i, i ^ bit) for i in range(lax.axis_size(axis...  24.9 us
    ppermute x9, waiting for transfers between devices, around(): return lax.ppermute(block, 'sp', route)  23.7 us
    pallas_call x8, Pallas kernels, expert_step(): pl.pallas_call(expert_kernel, out_shape=(jax.ShapeDtypeStruct((rows // pa...  15.2 us
    ppermute x9, starting transfers between devices, around(): return lax.ppermute(block, 'sp', route)  11.9 us
    dot_general x16, matrix products, matmul(): return jnp.dot(a, b, preferred_element_type=jnp.float32)  5.61 us
  transfers between devices with their start and end apart: 52, of which 27 were waited for; matrix products, arithmetic and copies ran while one was open for 6% of the time, Pallas kernels for 13%

profile of v3, /device:TPU:0, one launch (start us, length us, event | category | flops | bytes accessed | tf_op | source)
XLA Modules:
  0.0 193.2 jit_solution(14539460353468042123)
XLA Ops:
  1.4 3.1 %collective-permute-start.40 = (f32[128,4]{0,1:T(4,128)S(1)}, f32[128,4]{0,1:T(4,128)S(1)}, u32[]{:S(2)}, u32[]{:S(2)}) collective-permute-start(f32[128,4]{0,1:T(4,128)S(1)} %pad_maximum_fusion.4), channel_id=1, source_target_pairs={{0,8},{4,12},{16,0},{20,4},{24,16},{28,20},{8,24},{12,28},{1,9},{5... | collective-permute-start | bytes 6152 | tf_op jit(solution)/shard_map/ppermute | solution.py:35
  4.4 2.5 %collective-permute-start.28 = (f32[128,4]{0,1:T(4,128)S(1)}, f32[128,4]{0,1:T(4,128)S(1)}, u32[]{:S(2)}, u32[]{:S(2)}) collective-permute-start(f32[128,4]{0,1:T(4,128)S(1)} %pad_maximum_fusion.4), channel_id=1, source_target_pairs={{0,24},{4,28},{16,8},{20,12},{24,0},{28,4},{8,16},{12,20},{1,25},{... | collective-permute-start | bytes 6152 | tf_op jit(solution)/shard_map/ppermute | solution.py:35
  9.3 3.4 %collective-permute-start = (bf16[32,512]{1,0:T(8,128)(2,1)S(1)}, bf16[32,512]{1,0:T(8,128)(2,1)S(1)}, u32[]{:S(2)}, u32[]{:S(2)}) collective-permute-start(bf16[32,512]{1,0:T(8,128)(2,1)S(1)} %multiply_convert_fusion.1), channel_id=1, source_target_pairs={{0,4},{4,8},{8,12},{12,16},{16,20},{20,24},{24,28},{1,5},{5,9},{9,... | collective-permute-start | bytes 98312 | tf_op jit(solution)/shard_map/ppermute | solution.py:17
  15.2 3.8 %convolve.1 = (f32[512,512]{1,0:T(8,128)S(1)}, f32[512,128]{1,0:T(8,128)S(1)}, f32[512,128]{1,0:T(8,128)S(1)}, f32[31,512]{1,0:T(8,128)S(1)}, f32[1,512]{1,0:T(1,128)S(1)}) custom-call(bf16[512,512]{1,0:T(8,128)(2,1)S(1)} %multiply_convert_fusion.refs_0_.gated, f32[31,512]{1,0:T(8,128)} %refs_1_.1, f32[1,512]{1,0:T(1,128)} %bitcast.45), custom_call_target="tpu_custom_call" | custom-call | tf_op jit(solution)/shard_map/convolve/pallas_call | solution.py:167
  24.7 2.4 %fp.1 = (bf16[512,512]{1,0:T(8,128)(2,1)S(1)}, bf16[128,2048]{1,0:T(8,128)(2,1)S(1)}, f32[128,2048]{1,0:T(8,128)S(1)}) custom-call(s32[1]{0:T(128)} %bitcast.refs_0_, f32[512,512]{1,0:T(8,128)S(1)} %get-tuple-element.41.refs_1_, f32[32,512]{1,0:T(8,128)S(1)} %get-tuple-element.45.refs_2_, f32[1,512]{1,0:T(1,128)S(1)} %get-tuple-element.46.refs_3_, ...), custom_call_target="tpu_custom_call" | custom-call | tf_op jit(solution)/shard_map/fp/pallas_call | solution.py:254
  27.4 2.5 %lp.1 = (bf16[128,2048]{1,0:T(8,128)(2,1)S(1)}, f32[128,2048]{1,0:T(8,128)S(1)}) custom-call(s32[1]{0:T(128)} %bitcast.refs_0_, bf16[512,512]{1,0:T(8,128)(2,1)S(1)} %get-tuple-element.48.refs_1_, bf16[512,2048]{1,0:T(8,128)(2,1)} %refs_2_.1), custom_call_target="tpu_custom_call" | custom-call | tf_op jit(solution)/shard_map/lp/pallas_call | solution.py:266
  31.9 12.6 %collective-permute-done.6.from_chip = bf16[128,2048]{1,0:T(8,128)(2,1)S(1)} collective-permute-done((bf16[128,2048]{1,0:T(8,128)(2,1)S(1)}, bf16[128,2048]{1,0:T(8,128)(2,1)S(1)}, u32[]{:S(2)}, u32[]{:S(2)}) %collective-permute-start.6) | collective-permute-done | bytes 524320 | tf_op jit(solution)/shard_map/ppermute | solution.py:21
  48.0 5.1 %collective-permute-done.7 = bf16[64,2048]{1,0:T(8,128)(2,1)S(1)} collective-permute-done((bf16[64,2048]{1,0:T(8,128)(2,1)S(1)}, bf16[64,2048]{1,0:T(8,128)(2,1)S(1)}, u32[]{:S(2)}, u32[]{:S(2)}) %collective-permute-start.7) | collective-permute-done | bytes 262176 | tf_op jit(solution)/shard_map/ppermute | solution.py:21
  53.6 4.7 %collective-permute-done.17 = bf16[128,2048]{1,0:T(8,128)(2,1)S(1)} collective-permute-done((bf16[128,2048]{1,0:T(8,128)(2,1)S(1)}, bf16[128,2048]{1,0:T(8,128)(2,1)S(1)}, u32[]{:S(2)}, u32[]{:S(2)}) %collective-permute-start.17) | collective-permute-done | bytes 524320 | tf_op jit(solution)/shard_map/ppermute | solution.py:35
  62.1 3.3 %collective-permute-done.18 = bf16[64,2048]{1,0:T(8,128)(2,1)S(1)} collective-permute-done((bf16[64,2048]{1,0:T(8,128)(2,1)S(1)}, bf16[64,2048]{1,0:T(8,128)(2,1)S(1)}, u32[]{:S(2)}, u32[]{:S(2)}) %collective-permute-start.18) | collective-permute-done | bytes 262176 | tf_op jit(solution)/shard_map/ppermute | solution.py:21
  67.8 3.3 %collective-permute-done.29 = bf16[128,2048]{1,0:T(8,128)(2,1)S(1)} collective-permute-done((bf16[128,2048]{1,0:T(8,128)(2,1)S(1)}, bf16[128,2048]{1,0:T(8,128)(2,1)S(1)}, u32[]{:S(2)}, u32[]{:S(2)}) %collective-permute-start.29) | collective-permute-done | bytes 524320 | tf_op jit(solution)/shard_map/ppermute | solution.py:35
  80.3 4.3 %collective-permute-done.41 = bf16[128,2048]{1,0:T(8,128)(2,1)S(1)} collective-permute-done((bf16[128,2048]{1,0:T(8,128)(2,1)S(1)}, bf16[128,2048]{1,0:T(8,128)(2,1)S(1)}, u32[]{:S(2)}, u32[]{:S(2)}) %collective-permute-start.41) | collective-permute-done | bytes 524320 | tf_op jit(solution)/shard_map/ppermute | solution.py:35
  85.6 4.6 %collective-permute-done.31 = bf16[64,2048]{1,0:T(8,128)(2,1)S(1)} collective-permute-done((bf16[64,2048]{1,0:T(8,128)(2,1)S(1)}, bf16[64,2048]{1,0:T(8,128)(2,1)S(1)}, u32[]{:S(2)}, u32[]{:S(2)}) %collective-permute-start.31) | collective-permute-done | bytes 262176 | tf_op jit(solution)/shard_map/ppermute | solution.py:21
  96.7 3.2 %collective-permute-done.44 = bf16[64,2048]{1,0:T(8,128)(2,1)S(1)} collective-permute-done((bf16[64,2048]{1,0:T(8,128)(2,1)S(1)}, bf16[64,2048]{1,0:T(8,128)(2,1)S(1)}, u32[]{:S(2)}, u32[]{:S(2)}) %collective-permute-start.44) | collective-permute-done | bytes 262176 | tf_op jit(solution)/shard_map/ppermute | solution.py:21
  99.9 5.1 %collective-permute-done.43 = bf16[64,2048]{1,0:T(8,128)(2,1)S(1)} collective-permute-done((bf16[64,2048]{1,0:T(8,128)(2,1)S(1)}, bf16[64,2048]{1,0:T(8,128)(2,1)S(1)}, u32[]{:S(2)}, u32[]{:S(2)}) %collective-permute-start.43) | collective-permute-done | bytes 262176 | tf_op jit(solution)/shard_map/ppermute | solution.py:21
  110.4 8.1 %collective-permute-done.14 = bf16[64,2048]{1,0:T(8,128)(2,1)S(1)} collective-permute-done((bf16[64,2048]{1,0:T(8,128)(2,1)S(1)}, bf16[64,2048]{1,0:T(8,128)(2,1)S(1)}, u32[]{:S(2)}, u32[]{:S(2)}) %collective-permute-start.14) | collective-permute-done | bytes 262176 | tf_op jit(solution)/shard_map/ppermute | solution.py:21
  124.0 7.9 %collective-permute-done.25 = bf16[64,2048]{1,0:T(8,128)(2,1)S(1)} collective-permute-done((bf16[64,2048]{1,0:T(8,128)(2,1)S(1)}, bf16[64,2048]{1,0:T(8,128)(2,1)S(1)}, u32[]{:S(2)}, u32[]{:S(2)}) %collective-permute-start.25) | collective-permute-done | bytes 262176 | tf_op jit(solution)/shard_map/ppermute | solution.py:21
  132.7 6.7 %collective-permute-done.23 = bf16[64,2048]{1,0:T(8,128)(2,1)S(1)} collective-permute-done((bf16[64,2048]{1,0:T(8,128)(2,1)S(1)}, bf16[64,2048]{1,0:T(8,128)(2,1)S(1)}, u32[]{:S(2)}, u32[]{:S(2)}) %collective-permute-start.23) | collective-permute-done | bytes 262176 | tf_op jit(solution)/shard_map/ppermute | solution.py:21
  145.3 3.2 %collective-permute-done.26 = bf16[64,2048]{1,0:T(8,128)(2,1)S(1)} collective-permute-done((bf16[64,2048]{1,0:T(8,128)(2,1)S(1)}, bf16[64,2048]{1,0:T(8,128)(2,1)S(1)}, u32[]{:S(2)}, u32[]{:S(2)}) %collective-permute-start.26) | collective-permute-done | bytes 262176 | tf_op jit(solution)/shard_map/ppermute | solution.py:21
  150.5 4.7 %collective-permute-done.35 = bf16[64,2048]{1,0:T(8,128)(2,1)S(1)} collective-permute-done((bf16[64,2048]{1,0:T(8,128)(2,1)S(1)}, bf16[64,2048]{1,0:T(8,128)(2,1)S(1)}, u32[]{:S(2)}, u32[]{:S(2)}) %collective-permute-start.35) | collective-permute-done | bytes 262176 | tf_op jit(solution)/shard_map/ppermute | solution.py:21
  156.7 7.7 %collective-permute-done.38 = bf16[64,2048]{1,0:T(8,128)(2,1)S(1)} collective-permute-done((bf16[64,2048]{1,0:T(8,128)(2,1)S(1)}, bf16[64,2048]{1,0:T(8,128)(2,1)S(1)}, u32[]{:S(2)}, u32[]{:S(2)}) %collective-permute-start.38) | collective-permute-done | bytes 262176 | tf_op jit(solution)/shard_map/ppermute | solution.py:21
  167.0 6.5 %collective-permute-done.49 = bf16[64,2048]{1,0:T(8,128)(2,1)S(1)} collective-permute-done((bf16[64,2048]{1,0:T(8,128)(2,1)S(1)}, bf16[64,2048]{1,0:T(8,128)(2,1)S(1)}, u32[]{:S(2)}, u32[]{:S(2)}) %collective-permute-start.49) | collective-permute-done | bytes 262176 | tf_op jit(solution)/shard_map/ppermute | solution.py:21
  174.7 3.1 %collective-permute-done.47 = bf16[64,2048]{1,0:T(8,128)(2,1)S(1)} collective-permute-done((bf16[64,2048]{1,0:T(8,128)(2,1)S(1)}, bf16[64,2048]{1,0:T(8,128)(2,1)S(1)}, u32[]{:S(2)}, u32[]{:S(2)}) %collective-permute-start.47) | collective-permute-done | bytes 262176 | tf_op jit(solution)/shard_map/ppermute | solution.py:21
  181.5 10.4 %collective-permute-done.51.carried = bf16[128,2048]{1,0:T(8,128)(2,1)S(1)} collective-permute-done((bf16[128,2048]{1,0:T(8,128)(2,1)S(1)}, bf16[128,2048]{1,0:T(8,128)(2,1)S(1)}, u32[]{:S(2)}, u32[]{:S(2)}) %collective-permute-start.51) | collective-permute-done | bytes 524320 | tf_op jit(solution)/shard_map/ppermute | solution.py:35
  (164 shorter events, 70.2 us)
Async XLA Ops:
  1.4 17.6 %collective-permute-start.40 = (f32[128,4]{0,1:T(4,128)S(1)}, f32[128,4]{0,1:T(4,128)S(1)}, u32[]{:S(2)}, u32[]{:S(2)}) collective-permute-start(f32[128,4]{0,1:T(4,128)S(1)} %pad_maximum_fusion.4), channel_id=1, source_target_pairs={{0,8},{4,12},{16,0},{20,4},{24,16},{28,20},{8,24},{12,28},{1,9},{5... | collective-permute-start | bytes 6152 | tf_op jit(solution)/shard_map/ppermute | solution.py:35
  4.4 14.8 %collective-permute-start.28 = (f32[128,4]{0,1:T(4,128)S(1)}, f32[128,4]{0,1:T(4,128)S(1)}, u32[]{:S(2)}, u32[]{:S(2)}) collective-permute-start(f32[128,4]{0,1:T(4,128)S(1)} %pad_maximum_fusion.4), channel_id=1, source_target_pairs={{0,24},{4,28},{16,8},{20,12},{24,0},{28,4},{8,16},{12,20},{1,25},{... | collective-permute-start | bytes 6152 | tf_op jit(solution)/shard_map/ppermute | solution.py:35
  6.9 20.5 %collective-permute-start.16 = (f32[128,4]{0,1:T(4,128)S(1)}, f32[128,4]{0,1:T(4,128)S(1)}, u32[]{:S(2)}, u32[]{:S(2)}) collective-permute-start(f32[128,4]{0,1:T(4,128)S(1)} %pad_maximum_fusion.4), channel_id=1, source_target_pairs={{0,16},{4,20},{16,24},{20,28},{24,8},{28,12},{8,0},{12,4},{1,17},{... | collective-permute-start | bytes 6152 | tf_op jit(solution)/shard_map/ppermute | solution.py:35
  30.4 14.1 %collective-permute-start.6 = (bf16[128,2048]{1,0:T(8,128)(2,1)S(1)}, bf16[128,2048]{1,0:T(8,128)(2,1)S(1)}, u32[]{:S(2)}, u32[]{:S(2)}) collective-permute-start(bf16[128,2048]{1,0:T(8,128)(2,1)S(1)} %add_convert_fusion.3), channel_id=1, source_target_pairs={{0,2},{1,3},{2,0},{3,1},{4,6},{5,7},{6,4},{7,5},{8,10},{9,11},{10,... | collective-permute-start | bytes 1572872 | tf_op jit(solution)/shard_map/ppermute | solution.py:21
  45.0 13.2 %collective-permute-start.17 = (bf16[128,2048]{1,0:T(8,128)(2,1)S(1)}, bf16[128,2048]{1,0:T(8,128)(2,1)S(1)}, u32[]{:S(2)}, u32[]{:S(2)}) collective-permute-start(bf16[128,2048]{1,0:T(8,128)(2,1)S(1)} %hidden.1), channel_id=1, source_target_pairs={{0,16},{4,20},{16,24},{20,28},{24,8},{28,12},{8,0},{12,4},{1,17},{... | collective-permute-start | bytes 1572872 | tf_op jit(solution)/shard_map/ppermute | solution.py:35
  47.4 14.5 %collective-permute-start.9 = (bf16[64,2048]{1,0:T(8,128)(2,1)S(1)}, bf16[64,2048]{1,0:T(8,128)(2,1)S(1)}, u32[]{:S(2)}, u32[]{:S(2)}) collective-permute-start(bf16[64,2048]{1,0:T(8,128)(2,1)S(1)} %convolution_convert_fusion.6), channel_id=1, source_target_pairs={{0,2},{1,3},{2,0},{3,1},{4,6},{5,7},{6,4},{7,5},{8,10},{9,11},{10,... | collective-permute-start | bytes 786440 | tf_op jit(solution)/shard_map/ppermute | solution.py:21
  59.1 12.0 %collective-permute-start.29 = (bf16[128,2048]{1,0:T(8,128)(2,1)S(1)}, bf16[128,2048]{1,0:T(8,128)(2,1)S(1)}, u32[]{:S(2)}, u32[]{:S(2)}) collective-permute-start(bf16[128,2048]{1,0:T(8,128)(2,1)S(1)} %collective-permute-done.17), channel_id=1, source_target_pairs={{0,16},{4,20},{16,24},{20,28},{24,8},{28,12},{8,0},{12,4},{1,17},{... | collective-permute-start | bytes 1572872 | tf_op jit(solution)/shard_map/ppermute | solution.py:35
  61.3 14.0 %collective-permute-start.20 = (bf16[64,2048]{1,0:T(8,128)(2,1)S(1)}, bf16[64,2048]{1,0:T(8,128)(2,1)S(1)}, u32[]{:S(2)}, u32[]{:S(2)}) collective-permute-start(bf16[64,2048]{1,0:T(8,128)(2,1)S(1)} %convolution_convert_fusion.4), channel_id=1, source_target_pairs={{0,2},{1,3},{2,0},{3,1},{4,6},{5,7},{6,4},{7,5},{8,10},{9,11},{10,... | collective-permute-start | bytes 786440 | tf_op jit(solution)/shard_map/ppermute | solution.py:21
  62.0 32.7 %collective-permute-start.10 = (bf16[256,2048]{1,0:T(8,128)(2,1)S(1)}, bf16[256,2048]{1,0:T(8,128)(2,1)S(1)}, u32[]{:S(2)}, u32[]{:S(2)}) collective-permute-start(bf16[256,2048]{1,0:T(8,128)(2,1)S(1)} %pad_maximum_fusion.tokens), channel_id=1, source_target_pairs={{0,1},{1,0},{2,3},{3,2},{4,5},{5,4},{6,7},{7,6},{8,9},{9,8},{10,11... | collective-permute-start | bytes 3145736 | tf_op jit(solution)/shard_map/ppermute | solution.py:21
  75.4 31.8 %collective-permute-start.21 = (bf16[256,2048]{1,0:T(8,128)(2,1)S(1)}, bf16[256,2048]{1,0:T(8,128)(2,1)S(1)}, u32[]{:S(2)}, u32[]{:S(2)}) collective-permute-start(bf16[256,2048]{1,0:T(8,128)(2,1)S(1)} %pad_maximum_fusion.1.tokens), channel_id=1, source_target_pairs={{0,1},{1,0},{2,3},{3,2},{4,5},{5,4},{6,7},{7,6},{8,9},{9,8},{10,11... | collective-permute-start | bytes 3145736 | tf_op jit(solution)/shard_map/ppermute | solution.py:21
  77.9 12.3 %collective-permute-start.31 = (bf16[64,2048]{1,0:T(8,128)(2,1)S(1)}, bf16[64,2048]{1,0:T(8,128)(2,1)S(1)}, u32[]{:S(2)}, u32[]{:S(2)}) collective-permute-start(bf16[64,2048]{1,0:T(8,128)(2,1)S(1)} %collective-permute-done.30), channel_id=1, source_target_pairs={{0,2},{1,3},{2,0},{3,1},{4,6},{5,7},{6,4},{7,5},{8,10},{9,11},{10,... | collective-permute-start | bytes 786440 | tf_op jit(solution)/shard_map/ppermute | solution.py:21
  90.3 28.8 %collective-permute-start.33 = (bf16[256,2048]{1,0:T(8,128)(2,1)S(1)}, bf16[256,2048]{1,0:T(8,128)(2,1)S(1)}, u32[]{:S(2)}, u32[]{:S(2)}) collective-permute-start(bf16[256,2048]{1,0:T(8,128)(2,1)S(1)} %pad_maximum_fusion.2.tokens), channel_id=1, source_target_pairs={{0,1},{1,0},{2,3},{3,2},{4,5},{5,4},{6,7},{7,6},{8,9},{9,8},{10,11... | collective-permute-start | bytes 3145736 | tf_op jit(solution)/shard_map/ppermute | solution.py:21
  91.4 13.7 %collective-permute-start.43 = (bf16[64,2048]{1,0:T(8,128)(2,1)S(1)}, bf16[64,2048]{1,0:T(8,128)(2,1)S(1)}, u32[]{:S(2)}, u32[]{:S(2)}) collective-permute-start(bf16[64,2048]{1,0:T(8,128)(2,1)S(1)} %collective-permute-done.42), channel_id=1, source_target_pairs={{0,2},{1,3},{2,0},{3,1},{4,6},{5,7},{6,4},{7,5},{8,10},{9,11},{10,... | collective-permute-start | bytes 786440 | tf_op jit(solution)/shard_map/ppermute | solution.py:21
  96.6 13.2 %collective-permute-start.11 = (bf16[128,2048]{1,0:T(8,128)(2,1)S(1)}, bf16[128,2048]{1,0:T(8,128)(2,1)S(1)}, u32[]{:S(2)}, u32[]{:S(2)}) collective-permute-start(bf16[128,2048]{1,0:T(8,128)(2,1)S(1)} %get-tuple-element.54), channel_id=1, source_target_pairs={{0,1},{1,0},{2,3},{3,2},{4,5},{5,4},{6,7},{7,6},{8,9},{9,8},{10,11... | collective-permute-start | bytes 1572872 | tf_op jit(solution)/shard_map/ppermute | solution.py:21
  105.2 37.2 %collective-permute-start.45 = (bf16[256,2048]{1,0:T(8,128)(2,1)S(1)}, bf16[256,2048]{1,0:T(8,128)(2,1)S(1)}, u32[]{:S(2)}, u32[]{:S(2)}) collective-permute-start(bf16[256,2048]{1,0:T(8,128)(2,1)S(1)} %pad_maximum_fusion.3.tokens), channel_id=1, source_target_pairs={{0,1},{1,0},{2,3},{3,2},{4,5},{5,4},{6,7},{7,6},{8,9},{9,8},{10,11... | collective-permute-start | bytes 3145736 | tf_op jit(solution)/shard_map/ppermute | solution.py:21
  109.1 13.0 %collective-permute-start.24 = (bf16[128,2048]{1,0:T(8,128)(2,1)S(1)}, bf16[128,2048]{1,0:T(8,128)(2,1)S(1)}, u32[]{:S(2)}, u32[]{:S(2)}) collective-permute-start(bf16[128,2048]{1,0:T(8,128)(2,1)S(1)} %get-tuple-element.63), channel_id=1, source_target_pairs={{0,1},{1,0},{2,3},{3,2},{4,5},{5,4},{6,7},{7,6},{8,9},{9,8},{10,11... | collective-permute-start | bytes 1572872 | tf_op jit(solution)/shard_map/ppermute | solution.py:21
  109.7 12.6 %collective-permute-start.22 = (bf16[128,2048]{1,0:T(8,128)(2,1)S(1)}, bf16[128,2048]{1,0:T(8,128)(2,1)S(1)}, u32[]{:S(2)}, u32[]{:S(2)}) collective-permute-start(bf16[128,2048]{1,0:T(8,128)(2,1)S(1)} %get-tuple-element.60), channel_id=1, source_target_pairs={{0,1},{1,0},{2,3},{3,2},{4,5},{5,4},{6,7},{7,6},{8,9},{9,8},{10,11... | collective-permute-start | bytes 1572872 | tf_op jit(solution)/shard_map/ppermute | solution.py:21
  118.5 62.6 %collective-permute-start.12 = (bf16[64,2048]{1,0:T(8,128)(2,1)S(1)}, bf16[64,2048]{1,0:T(8,128)(2,1)S(1)}, u32[]{:S(2)}, u32[]{:S(2)}) collective-permute-start(bf16[64,2048]{1,0:T(8,128)(2,1)S(1)} %add_convert_fusion.19), channel_id=1, source_target_pairs={{0,2},{1,3},{2,0},{3,1},{4,6},{5,7},{6,4},{7,5},{8,10},{9,11},{10,... | collective-permute-start | bytes 786440 | tf_op jit(solution)/shard_map/ppermute | solution.py:21
  119.1 61.7 %collective-permute-start.15 = (bf16[64,2048]{1,0:T(8,128)(2,1)S(1)}, bf16[64,2048]{1,0:T(8,128)(2,1)S(1)}, u32[]{:S(2)}, u32[]{:S(2)}) collective-permute-start(bf16[64,2048]{1,0:T(8,128)(2,1)S(1)} %add_convert_fusion.16), channel_id=1, source_target_pairs={{0,4},{4,0},{8,12},{12,8},{16,20},{20,16},{24,28},{28,24},{1,5},{5... | collective-permute-start | bytes 786440 | tf_op jit(solution)/shard_map/ppermute | solution.py:21
  122.1 17.6 %collective-permute-start.36 = (bf16[128,2048]{1,0:T(8,128)(2,1)S(1)}, bf16[128,2048]{1,0:T(8,128)(2,1)S(1)}, u32[]{:S(2)}, u32[]{:S(2)}) collective-permute-start(bf16[128,2048]{1,0:T(8,128)(2,1)S(1)} %get-tuple-element.69), channel_id=1, source_target_pairs={{0,1},{1,0},{2,3},{3,2},{4,5},{5,4},{6,7},{7,6},{8,9},{9,8},{10,11... | collective-permute-start | bytes 1572872 | tf_op jit(solution)/shard_map/ppermute | solution.py:21
  142.4 12.8 %collective-permute-start.35 = (bf16[64,2048]{1,0:T(8,128)(2,1)S(1)}, bf16[64,2048]{1,0:T(8,128)(2,1)S(1)}, u32[]{:S(2)}, u32[]{:S(2)}) collective-permute-start(bf16[64,2048]{1,0:T(8,128)(2,1)S(1)} %add_convert_fusion.11), channel_id=1, source_target_pairs={{0,2},{1,3},{2,0},{3,1},{4,6},{5,7},{6,4},{7,5},{8,10},{9,11},{10,... | collective-permute-start | bytes 786440 | tf_op jit(solution)/shard_map/ppermute | solution.py:21
  150.4 15.0 %collective-permute-start.27 = (bf16[128,2048]{1,0:T(8,128)(2,1)S(1)}, bf16[128,2048]{1,0:T(8,128)(2,1)S(1)}, u32[]{:S(2)}, u32[]{:S(2)}) collective-permute-start(bf16[128,2048]{1,0:T(8,128)(2,1)S(1)} %add_convert_fusion.2), channel_id=1, source_target_pairs={{0,16},{4,20},{16,24},{20,28},{24,8},{28,12},{8,0},{12,4},{1,17},{... | collective-permute-start | bytes 1572872 | tf_op jit(solution)/shard_map/ppermute | solution.py:35
  165.9 13.2 %collective-permute-start.39 = (bf16[128,2048]{1,0:T(8,128)(2,1)S(1)}, bf16[128,2048]{1,0:T(8,128)(2,1)S(1)}, u32[]{:S(2)}, u32[]{:S(2)}) collective-permute-start(bf16[128,2048]{1,0:T(8,128)(2,1)S(1)} %add_convert_fusion.1), channel_id=1, source_target_pairs={{0,16},{4,20},{16,24},{20,28},{24,8},{28,12},{8,0},{12,4},{1,17},{... | collective-permute-start | bytes 1572872 | tf_op jit(solution)/shard_map/ppermute | solution.py:35
  166.0 11.8 %collective-permute-start.47 = (bf16[64,2048]{1,0:T(8,128)(2,1)S(1)}, bf16[64,2048]{1,0:T(8,128)(2,1)S(1)}, u32[]{:S(2)}, u32[]{:S(2)}) collective-permute-start(bf16[64,2048]{1,0:T(8,128)(2,1)S(1)} %add_convert_fusion.7), channel_id=1, source_target_pairs={{0,2},{1,3},{2,0},{3,1},{4,6},{5,7},{6,4},{7,5},{8,10},{9,11},{10,... | collective-permute-start | bytes 786440 | tf_op jit(solution)/shard_map/ppermute | solution.py:21
  (34 other events, 313.5 us)

commit v4 on v3

--- a/solution.py
+++ b/solution.py
@@ -131,19 +131,19 @@
     first = pad - (taps.shape[0] - 1)
     extended[0:pad, :] = before[...].astype(jnp.float32)
     extended[pad : 2 * pad, :] = gated[0:pad, :].astype(jnp.float32)
-    total[0:pad, :] = jnp.zeros((pad, 128), jnp.float32)
-    squares[0:pad, :] = jnp.zeros((pad, 128), jnp.float32)
+    own_total = jnp.zeros((pad, 128), jnp.float32)
+    own_squares = jnp.zeros((pad, 128), jnp.float32)
     for lane in range(0, channels, 128):
         window = slice(lane, lane + 128)
         sums = convolve_rows(extended, taps, first, 0, pad, window)
         head[:, window] = sums
-        total[0:pad, :] += sums
-        squares[0:pad, :] += sums * sums
+        own_total = own_total + sums
+        own_squares = own_squares + sums * sums
     ones = jnp.ones((8, 128), jnp.float32)
-    for place, partial in enumerate((total, squares)):
+    for place, (own, partial) in enumerate(((own_total, total), (own_squares, squares))):
         sums = lax.dot_general(
             ones,
-            partial[...],
+            jnp.concatenate([own, partial[pad:, :]], axis=0),
             (((1,), (1,)), ((), ())),
             precision=lax.Precision.HIGHEST,
             preferred_element_type=jnp.float32,

time: 194 us -> 194 us (level)
  no operation moved by 1% of the time
where the time goes in v4:
time: 194 us; the launch traced here: 193 us
  waiting for transfers between devices  114 us (59%)
  starting transfers between devices  40.1 us (21%)
  Pallas kernels  26.3 us (14%)
  other arithmetic  6.57 us (3%)
  matrix products  5.61 us (3%)
    ppermute x42, waiting for transfers between devices, swapped(): lax.ppermute(block, axis, [(i, i ^ bit) for i in range(lax.axis_size(axis...  90.1 us
    ppermute x42, starting transfers between devices, swapped(): lax.ppermute(block, axis, [(i, i ^ bit) for i in range(lax.axis_size(axis...  24.9 us
    ppermute x9, waiting for transfers between devices, around(): return lax.ppermute(block, 'sp', route)  23.8 us
    pallas_call x8, Pallas kernels, expert_step(): pl.pallas_call(expert_kernel, out_shape=(jax.ShapeDtypeStruct((rows // pa...  15.3 us
    ppermute x9, starting transfers between devices, around(): return lax.ppermute(block, 'sp', route)  11.8 us
    dot_general x16, matrix products, matmul(): return jnp.dot(a, b, preferred_element_type=jnp.float32)  5.61 us
  transfers between devices with their start and end apart: 52, of which 27 were waited for; matrix products, arithmetic and copies ran while one was open for 6% of the time, Pallas kernels for 13%

profile of v4, /device:TPU:0, one launch (start us, length us, event | category | flops | bytes accessed | tf_op | source)
XLA Modules:
  0.0 193.1 jit_solution(144163420630409743)
XLA Ops:
  1.4 3.1 %collective-permute-start.40 = (f32[128,4]{0,1:T(4,128)S(1)}, f32[128,4]{0,1:T(4,128)S(1)}, u32[]{:S(2)}, u32[]{:S(2)}) collective-permute-start(f32[128,4]{0,1:T(4,128)S(1)} %pad_maximum_fusion.4), channel_id=1, source_target_pairs={{0,8},{4,12},{16,0},{20,4},{24,16},{28,20},{8,24},{12,28},{1,9},{5... | collective-permute-start | bytes 6152 | tf_op jit(solution)/shard_map/ppermute | solution.py:35
  4.4 2.5 %collective-permute-start.28 = (f32[128,4]{0,1:T(4,128)S(1)}, f32[128,4]{0,1:T(4,128)S(1)}, u32[]{:S(2)}, u32[]{:S(2)}) collective-permute-start(f32[128,4]{0,1:T(4,128)S(1)} %pad_maximum_fusion.4), channel_id=1, source_target_pairs={{0,24},{4,28},{16,8},{20,12},{24,0},{28,4},{8,16},{12,20},{1,25},{... | collective-permute-start | bytes 6152 | tf_op jit(solution)/shard_map/ppermute | solution.py:35
  9.3 3.4 %collective-permute-start = (bf16[32,512]{1,0:T(8,128)(2,1)S(1)}, bf16[32,512]{1,0:T(8,128)(2,1)S(1)}, u32[]{:S(2)}, u32[]{:S(2)}) collective-permute-start(bf16[32,512]{1,0:T(8,128)(2,1)S(1)} %multiply_convert_fusion.1), channel_id=1, source_target_pairs={{0,4},{4,8},{8,12},{12,16},{16,20},{20,24},{24,28},{1,5},{5,9},{9,... | collective-permute-start | bytes 98312 | tf_op jit(solution)/shard_map/ppermute | solution.py:17
  15.2 3.8 %convolve.1 = (f32[512,512]{1,0:T(8,128)S(1)}, f32[512,128]{1,0:T(8,128)S(1)}, f32[512,128]{1,0:T(8,128)S(1)}, f32[31,512]{1,0:T(8,128)S(1)}, f32[1,512]{1,0:T(1,128)S(1)}) custom-call(bf16[512,512]{1,0:T(8,128)(2,1)S(1)} %multiply_convert_fusion.refs_0_.gated, f32[31,512]{1,0:T(8,128)} %refs_1_.1, f32[1,512]{1,0:T(1,128)} %bitcast.45), custom_call_target="tpu_custom_call" | custom-call | tf_op jit(solution)/shard_map/convolve/pallas_call | solution.py:167
  24.7 2.4 %fp.1 = (bf16[512,512]{1,0:T(8,128)(2,1)S(1)}, bf16[128,2048]{1,0:T(8,128)(2,1)S(1)}, f32[128,2048]{1,0:T(8,128)S(1)}) custom-call(s32[1]{0:T(128)} %bitcast.refs_0_, f32[512,512]{1,0:T(8,128)S(1)} %get-tuple-element.41.refs_1_, f32[32,512]{1,0:T(8,128)S(1)} %get-tuple-element.45.refs_2_, f32[1,512]{1,0:T(1,128)S(1)} %get-tuple-element.46.refs_3_, ...), custom_call_target="tpu_custom_call" | custom-call | tf_op jit(solution)/shard_map/fp/pallas_call | solution.py:254
  27.5 2.4 %lp.1 = (bf16[128,2048]{1,0:T(8,128)(2,1)S(1)}, f32[128,2048]{1,0:T(8,128)S(1)}) custom-call(s32[1]{0:T(128)} %bitcast.refs_0_, bf16[512,512]{1,0:T(8,128)(2,1)S(1)} %get-tuple-element.48.refs_1_, bf16[512,2048]{1,0:T(8,128)(2,1)} %refs_2_.1), custom_call_target="tpu_custom_call" | custom-call | tf_op jit(solution)/shard_map/lp/pallas_call | solution.py:266
  31.9 12.6 %collective-permute-done.6.from_chip = bf16[128,2048]{1,0:T(8,128)(2,1)S(1)} collective-permute-done((bf16[128,2048]{1,0:T(8,128)(2,1)S(1)}, bf16[128,2048]{1,0:T(8,128)(2,1)S(1)}, u32[]{:S(2)}, u32[]{:S(2)}) %collective-permute-start.6) | collective-permute-done | bytes 524320 | tf_op jit(solution)/shard_map/ppermute | solution.py:21
  48.0 5.1 %collective-permute-done.7 = bf16[64,2048]{1,0:T(8,128)(2,1)S(1)} collective-permute-done((bf16[64,2048]{1,0:T(8,128)(2,1)S(1)}, bf16[64,2048]{1,0:T(8,128)(2,1)S(1)}, u32[]{:S(2)}, u32[]{:S(2)}) %collective-permute-start.7) | collective-permute-done | bytes 262176 | tf_op jit(solution)/shard_map/ppermute | solution.py:21
  53.6 4.7 %collective-permute-done.17 = bf16[128,2048]{1,0:T(8,128)(2,1)S(1)} collective-permute-done((bf16[128,2048]{1,0:T(8,128)(2,1)S(1)}, bf16[128,2048]{1,0:T(8,128)(2,1)S(1)}, u32[]{:S(2)}, u32[]{:S(2)}) %collective-permute-start.17) | collective-permute-done | bytes 524320 | tf_op jit(solution)/shard_map/ppermute | solution.py:35
  62.0 3.3 %collective-permute-done.18 = bf16[64,2048]{1,0:T(8,128)(2,1)S(1)} collective-permute-done((bf16[64,2048]{1,0:T(8,128)(2,1)S(1)}, bf16[64,2048]{1,0:T(8,128)(2,1)S(1)}, u32[]{:S(2)}, u32[]{:S(2)}) %collective-permute-start.18) | collective-permute-done | bytes 262176 | tf_op jit(solution)/shard_map/ppermute | solution.py:21
  67.7 3.4 %collective-permute-done.29 = bf16[128,2048]{1,0:T(8,128)(2,1)S(1)} collective-permute-done((bf16[128,2048]{1,0:T(8,128)(2,1)S(1)}, bf16[128,2048]{1,0:T(8,128)(2,1)S(1)}, u32[]{:S(2)}, u32[]{:S(2)}) %collective-permute-start.29) | collective-permute-done | bytes 524320 | tf_op jit(solution)/shard_map/ppermute | solution.py:35
  80.2 4.3 %collective-permute-done.41 = bf16[128,2048]{1,0:T(8,128)(2,1)S(1)} collective-permute-done((bf16[128,2048]{1,0:T(8,128)(2,1)S(1)}, bf16[128,2048]{1,0:T(8,128)(2,1)S(1)}, u32[]{:S(2)}, u32[]{:S(2)}) %collective-permute-start.41) | collective-permute-done | bytes 524320 | tf_op jit(solution)/shard_map/ppermute | solution.py:35
  85.5 4.7 %collective-permute-done.31 = bf16[64,2048]{1,0:T(8,128)(2,1)S(1)} collective-permute-done((bf16[64,2048]{1,0:T(8,128)(2,1)S(1)}, bf16[64,2048]{1,0:T(8,128)(2,1)S(1)}, u32[]{:S(2)}, u32[]{:S(2)}) %collective-permute-start.31) | collective-permute-done | bytes 262176 | tf_op jit(solution)/shard_map/ppermute | solution.py:21
  96.7 3.2 %collective-permute-done.44 = bf16[64,2048]{1,0:T(8,128)(2,1)S(1)} collective-permute-done((bf16[64,2048]{1,0:T(8,128)(2,1)S(1)}, bf16[64,2048]{1,0:T(8,128)(2,1)S(1)}, u32[]{:S(2)}, u32[]{:S(2)}) %collective-permute-start.44) | collective-permute-done | bytes 262176 | tf_op jit(solution)/shard_map/ppermute | solution.py:21
  99.9 5.1 %collective-permute-done.43 = bf16[64,2048]{1,0:T(8,128)(2,1)S(1)} collective-permute-done((bf16[64,2048]{1,0:T(8,128)(2,1)S(1)}, bf16[64,2048]{1,0:T(8,128)(2,1)S(1)}, u32[]{:S(2)}, u32[]{:S(2)}) %collective-permute-start.43) | collective-permute-done | bytes 262176 | tf_op jit(solution)/shard_map/ppermute | solution.py:21
  110.3 8.1 %collective-permute-done.14 = bf16[64,2048]{1,0:T(8,128)(2,1)S(1)} collective-permute-done((bf16[64,2048]{1,0:T(8,128)(2,1)S(1)}, bf16[64,2048]{1,0:T(8,128)(2,1)S(1)}, u32[]{:S(2)}, u32[]{:S(2)}) %collective-permute-start.14) | collective-permute-done | bytes 262176 | tf_op jit(solution)/shard_map/ppermute | solution.py:21
  123.9 7.9 %collective-permute-done.25 = bf16[64,2048]{1,0:T(8,128)(2,1)S(1)} collective-permute-done((bf16[64,2048]{1,0:T(8,128)(2,1)S(1)}, bf16[64,2048]{1,0:T(8,128)(2,1)S(1)}, u32[]{:S(2)}, u32[]{:S(2)}) %collective-permute-start.25) | collective-permute-done | bytes 262176 | tf_op jit(solution)/shard_map/ppermute | solution.py:21
  132.7 6.7 %collective-permute-done.23 = bf16[64,2048]{1,0:T(8,128)(2,1)S(1)} collective-permute-done((bf16[64,2048]{1,0:T(8,128)(2,1)S(1)}, bf16[64,2048]{1,0:T(8,128)(2,1)S(1)}, u32[]{:S(2)}, u32[]{:S(2)}) %collective-permute-start.23) | collective-permute-done | bytes 262176 | tf_op jit(solution)/shard_map/ppermute | solution.py:21
  145.3 3.2 %collective-permute-done.26 = bf16[64,2048]{1,0:T(8,128)(2,1)S(1)} collective-permute-done((bf16[64,2048]{1,0:T(8,128)(2,1)S(1)}, bf16[64,2048]{1,0:T(8,128)(2,1)S(1)}, u32[]{:S(2)}, u32[]{:S(2)}) %collective-permute-start.26) | collective-permute-done | bytes 262176 | tf_op jit(solution)/shard_map/ppermute | solution.py:21
  150.5 4.7 %collective-permute-done.35 = bf16[64,2048]{1,0:T(8,128)(2,1)S(1)} collective-permute-done((bf16[64,2048]{1,0:T(8,128)(2,1)S(1)}, bf16[64,2048]{1,0:T(8,128)(2,1)S(1)}, u32[]{:S(2)}, u32[]{:S(2)}) %collective-permute-start.35) | collective-permute-done | bytes 262176 | tf_op jit(solution)/shard_map/ppermute | solution.py:21
  156.7 7.7 %collective-permute-done.38 = bf16[64,2048]{1,0:T(8,128)(2,1)S(1)} collective-permute-done((bf16[64,2048]{1,0:T(8,128)(2,1)S(1)}, bf16[64,2048]{1,0:T(8,128)(2,1)S(1)}, u32[]{:S(2)}, u32[]{:S(2)}) %collective-permute-start.38) | collective-permute-done | bytes 262176 | tf_op jit(solution)/shard_map/ppermute | solution.py:21
  167.0 6.5 %collective-permute-done.49 = bf16[64,2048]{1,0:T(8,128)(2,1)S(1)} collective-permute-done((bf16[64,2048]{1,0:T(8,128)(2,1)S(1)}, bf16[64,2048]{1,0:T(8,128)(2,1)S(1)}, u32[]{:S(2)}, u32[]{:S(2)}) %collective-permute-start.49) | collective-permute-done | bytes 262176 | tf_op jit(solution)/shard_map/ppermute | solution.py:21
  174.7 3.1 %collective-permute-done.47 = bf16[64,2048]{1,0:T(8,128)(2,1)S(1)} collective-permute-done((bf16[64,2048]{1,0:T(8,128)(2,1)S(1)}, bf16[64,2048]{1,0:T(8,128)(2,1)S(1)}, u32[]{:S(2)}, u32[]{:S(2)}) %collective-permute-start.47) | collective-permute-done | bytes 262176 | tf_op jit(solution)/shard_map/ppermute | solution.py:21
  181.5 10.4 %collective-permute-done.51.carried = bf16[128,2048]{1,0:T(8,128)(2,1)S(1)} collective-permute-done((bf16[128,2048]{1,0:T(8,128)(2,1)S(1)}, bf16[128,2048]{1,0:T(8,128)(2,1)S(1)}, u32[]{:S(2)}, u32[]{:S(2)}) %collective-permute-start.51) | collective-permute-done | bytes 524320 | tf_op jit(solution)/shard_map/ppermute | solution.py:35
  (164 shorter events, 70.1 us)
Async XLA Ops:
  1.4 17.6 %collective-permute-start.40 = (f32[128,4]{0,1:T(4,128)S(1)}, f32[128,4]{0,1:T(4,128)S(1)}, u32[]{:S(2)}, u32[]{:S(2)}) collective-permute-start(f32[128,4]{0,1:T(4,128)S(1)} %pad_maximum_fusion.4), channel_id=1, source_target_pairs={{0,8},{4,12},{16,0},{20,4},{24,16},{28,20},{8,24},{12,28},{1,9},{5... | collective-permute-start | bytes 6152 | tf_op jit(solution)/shard_map/ppermute | solution.py:35
  4.4 14.8 %collective-permute-start.28 = (f32[128,4]{0,1:T(4,128)S(1)}, f32[128,4]{0,1:T(4,128)S(1)}, u32[]{:S(2)}, u32[]{:S(2)}) collective-permute-start(f32[128,4]{0,1:T(4,128)S(1)} %pad_maximum_fusion.4), channel_id=1, source_target_pairs={{0,24},{4,28},{16,8},{20,12},{24,0},{28,4},{8,16},{12,20},{1,25},{... | collective-permute-start | bytes 6152 | tf_op jit(solution)/shard_map/ppermute | solution.py:35
  6.9 20.5 %collective-permute-start.16 = (f32[128,4]{0,1:T(4,128)S(1)}, f32[128,4]{0,1:T(4,128)S(1)}, u32[]{:S(2)}, u32[]{:S(2)}) collective-permute-start(f32[128,4]{0,1:T(4,128)S(1)} %pad_maximum_fusion.4), channel_id=1, source_target_pairs={{0,16},{4,20},{16,24},{20,28},{24,8},{28,12},{8,0},{12,4},{1,17},{... | collective-permute-start | bytes 6152 | tf_op jit(solution)/shard_map/ppermute | solution.py:35
  30.4 14.1 %collective-permute-start.6 = (bf16[128,2048]{1,0:T(8,128)(2,1)S(1)}, bf16[128,2048]{1,0:T(8,128)(2,1)S(1)}, u32[]{:S(2)}, u32[]{:S(2)}) collective-permute-start(bf16[128,2048]{1,0:T(8,128)(2,1)S(1)} %add_convert_fusion.3), channel_id=1, source_target_pairs={{0,2},{1,3},{2,0},{3,1},{4,6},{5,7},{6,4},{7,5},{8,10},{9,11},{10,... | collective-permute-start | bytes 1572872 | tf_op jit(solution)/shard_map/ppermute | solution.py:21
  45.0 13.2 %collective-permute-start.17 = (bf16[128,2048]{1,0:T(8,128)(2,1)S(1)}, bf16[128,2048]{1,0:T(8,128)(2,1)S(1)}, u32[]{:S(2)}, u32[]{:S(2)}) collective-permute-start(bf16[128,2048]{1,0:T(8,128)(2,1)S(1)} %hidden.1), channel_id=1, source_target_pairs={{0,16},{4,20},{16,24},{20,28},{24,8},{28,12},{8,0},{12,4},{1,17},{... | collective-permute-start | bytes 1572872 | tf_op jit(solution)/shard_map/ppermute | solution.py:35
  47.4 14.5 %collective-permute-start.9 = (bf16[64,2048]{1,0:T(8,128)(2,1)S(1)}, bf16[64,2048]{1,0:T(8,128)(2,1)S(1)}, u32[]{:S(2)}, u32[]{:S(2)}) collective-permute-start(bf16[64,2048]{1,0:T(8,128)(2,1)S(1)} %convolution_convert_fusion.6), channel_id=1, source_target_pairs={{0,2},{1,3},{2,0},{3,1},{4,6},{5,7},{6,4},{7,5},{8,10},{9,11},{10,... | collective-permute-start | bytes 786440 | tf_op jit(solution)/shard_map/ppermute | solution.py:21
  59.1 12.0 %collective-permute-start.29 = (bf16[128,2048]{1,0:T(8,128)(2,1)S(1)}, bf16[128,2048]{1,0:T(8,128)(2,1)S(1)}, u32[]{:S(2)}, u32[]{:S(2)}) collective-permute-start(bf16[128,2048]{1,0:T(8,128)(2,1)S(1)} %collective-permute-done.17), channel_id=1, source_target_pairs={{0,16},{4,20},{16,24},{20,28},{24,8},{28,12},{8,0},{12,4},{1,17},{... | collective-permute-start | bytes 1572872 | tf_op jit(solution)/shard_map/ppermute | solution.py:35
  61.3 13.9 %collective-permute-start.20 = (bf16[64,2048]{1,0:T(8,128)(2,1)S(1)}, bf16[64,2048]{1,0:T(8,128)(2,1)S(1)}, u32[]{:S(2)}, u32[]{:S(2)}) collective-permute-start(bf16[64,2048]{1,0:T(8,128)(2,1)S(1)} %convolution_convert_fusion.4), channel_id=1, source_target_pairs={{0,2},{1,3},{2,0},{3,1},{4,6},{5,7},{6,4},{7,5},{8,10},{9,11},{10,... | collective-permute-start | bytes 786440 | tf_op jit(solution)/shard_map/ppermute | solution.py:21
  62.0 32.7 %collective-permute-start.10 = (bf16[256,2048]{1,0:T(8,128)(2,1)S(1)}, bf16[256,2048]{1,0:T(8,128)(2,1)S(1)}, u32[]{:S(2)}, u32[]{:S(2)}) collective-permute-start(bf16[256,2048]{1,0:T(8,128)(2,1)S(1)} %pad_maximum_fusion.tokens), channel_id=1, source_target_pairs={{0,1},{1,0},{2,3},{3,2},{4,5},{5,4},{6,7},{7,6},{8,9},{9,8},{10,11... | collective-permute-start | bytes 3145736 | tf_op jit(solution)/shard_map/ppermute | solution.py:21
  75.4 31.8 %collective-permute-start.21 = (bf16[256,2048]{1,0:T(8,128)(2,1)S(1)}, bf16[256,2048]{1,0:T(8,128)(2,1)S(1)}, u32[]{:S(2)}, u32[]{:S(2)}) collective-permute-start(bf16[256,2048]{1,0:T(8,128)(2,1)S(1)} %pad_maximum_fusion.1.tokens), channel_id=1, source_target_pairs={{0,1},{1,0},{2,3},{3,2},{4,5},{5,4},{6,7},{7,6},{8,9},{9,8},{10,11... | collective-permute-start | bytes 3145736 | tf_op jit(solution)/shard_map/ppermute | solution.py:21
  77.9 12.3 %collective-permute-start.31 = (bf16[64,2048]{1,0:T(8,128)(2,1)S(1)}, bf16[64,2048]{1,0:T(8,128)(2,1)S(1)}, u32[]{:S(2)}, u32[]{:S(2)}) collective-permute-start(bf16[64,2048]{1,0:T(8,128)(2,1)S(1)} %collective-permute-done.30), channel_id=1, source_target_pairs={{0,2},{1,3},{2,0},{3,1},{4,6},{5,7},{6,4},{7,5},{8,10},{9,11},{10,... | collective-permute-start | bytes 786440 | tf_op jit(solution)/shard_map/ppermute | solution.py:21
  90.2 28.8 %collective-permute-start.33 = (bf16[256,2048]{1,0:T(8,128)(2,1)S(1)}, bf16[256,2048]{1,0:T(8,128)(2,1)S(1)}, u32[]{:S(2)}, u32[]{:S(2)}) collective-permute-start(bf16[256,2048]{1,0:T(8,128)(2,1)S(1)} %pad_maximum_fusion.2.tokens), channel_id=1, source_target_pairs={{0,1},{1,0},{2,3},{3,2},{4,5},{5,4},{6,7},{7,6},{8,9},{9,8},{10,11... | collective-permute-start | bytes 3145736 | tf_op jit(solution)/shard_map/ppermute | solution.py:21
  91.3 13.7 %collective-permute-start.43 = (bf16[64,2048]{1,0:T(8,128)(2,1)S(1)}, bf16[64,2048]{1,0:T(8,128)(2,1)S(1)}, u32[]{:S(2)}, u32[]{:S(2)}) collective-permute-start(bf16[64,2048]{1,0:T(8,128)(2,1)S(1)} %collective-permute-done.42), channel_id=1, source_target_pairs={{0,2},{1,3},{2,0},{3,1},{4,6},{5,7},{6,4},{7,5},{8,10},{9,11},{10,... | collective-permute-start | bytes 786440 | tf_op jit(solution)/shard_map/ppermute | solution.py:21
  96.6 13.2 %collective-permute-start.11 = (bf16[128,2048]{1,0:T(8,128)(2,1)S(1)}, bf16[128,2048]{1,0:T(8,128)(2,1)S(1)}, u32[]{:S(2)}, u32[]{:S(2)}) collective-permute-start(bf16[128,2048]{1,0:T(8,128)(2,1)S(1)} %get-tuple-element.54), channel_id=1, source_target_pairs={{0,1},{1,0},{2,3},{3,2},{4,5},{5,4},{6,7},{7,6},{8,9},{9,8},{10,11... | collective-permute-start | bytes 1572872 | tf_op jit(solution)/shard_map/ppermute | solution.py:21
  105.1 37.2 %collective-permute-start.45 = (bf16[256,2048]{1,0:T(8,128)(2,1)S(1)}, bf16[256,2048]{1,0:T(8,128)(2,1)S(1)}, u32[]{:S(2)}, u32[]{:S(2)}) collective-permute-start(bf16[256,2048]{1,0:T(8,128)(2,1)S(1)} %pad_maximum_fusion.3.tokens), channel_id=1, source_target_pairs={{0,1},{1,0},{2,3},{3,2},{4,5},{5,4},{6,7},{7,6},{8,9},{9,8},{10,11... | collective-permute-start | bytes 3145736 | tf_op jit(solution)/shard_map/ppermute | solution.py:21
  109.1 13.0 %collective-permute-start.24 = (bf16[128,2048]{1,0:T(8,128)(2,1)S(1)}, bf16[128,2048]{1,0:T(8,128)(2,1)S(1)}, u32[]{:S(2)}, u32[]{:S(2)}) collective-permute-start(bf16[128,2048]{1,0:T(8,128)(2,1)S(1)} %get-tuple-element.63), channel_id=1, source_target_pairs={{0,1},{1,0},{2,3},{3,2},{4,5},{5,4},{6,7},{7,6},{8,9},{9,8},{10,11... | collective-permute-start | bytes 1572872 | tf_op jit(solution)/shard_map/ppermute | solution.py:21
  109.6 12.6 %collective-permute-start.22 = (bf16[128,2048]{1,0:T(8,128)(2,1)S(1)}, bf16[128,2048]{1,0:T(8,128)(2,1)S(1)}, u32[]{:S(2)}, u32[]{:S(2)}) collective-permute-start(bf16[128,2048]{1,0:T(8,128)(2,1)S(1)} %get-tuple-element.60), channel_id=1, source_target_pairs={{0,1},{1,0},{2,3},{3,2},{4,5},{5,4},{6,7},{7,6},{8,9},{9,8},{10,11... | collective-permute-start | bytes 1572872 | tf_op jit(solution)/shard_map/ppermute | solution.py:21
  118.5 62.6 %collective-permute-start.12 = (bf16[64,2048]{1,0:T(8,128)(2,1)S(1)}, bf16[64,2048]{1,0:T(8,128)(2,1)S(1)}, u32[]{:S(2)}, u32[]{:S(2)}) collective-permute-start(bf16[64,2048]{1,0:T(8,128)(2,1)S(1)} %add_convert_fusion.19), channel_id=1, source_target_pairs={{0,2},{1,3},{2,0},{3,1},{4,6},{5,7},{6,4},{7,5},{8,10},{9,11},{10,... | collective-permute-start | bytes 786440 | tf_op jit(solution)/shard_map/ppermute | solution.py:21
  119.0 61.7 %collective-permute-start.15 = (bf16[64,2048]{1,0:T(8,128)(2,1)S(1)}, bf16[64,2048]{1,0:T(8,128)(2,1)S(1)}, u32[]{:S(2)}, u32[]{:S(2)}) collective-permute-start(bf16[64,2048]{1,0:T(8,128)(2,1)S(1)} %add_convert_fusion.16), channel_id=1, source_target_pairs={{0,4},{4,0},{8,12},{12,8},{16,20},{20,16},{24,28},{28,24},{1,5},{5... | collective-permute-start | bytes 786440 | tf_op jit(solution)/shard_map/ppermute | solution.py:21
  122.1 17.6 %collective-permute-start.36 = (bf16[128,2048]{1,0:T(8,128)(2,1)S(1)}, bf16[128,2048]{1,0:T(8,128)(2,1)S(1)}, u32[]{:S(2)}, u32[]{:S(2)}) collective-permute-start(bf16[128,2048]{1,0:T(8,128)(2,1)S(1)} %get-tuple-element.69), channel_id=1, source_target_pairs={{0,1},{1,0},{2,3},{3,2},{4,5},{5,4},{6,7},{7,6},{8,9},{9,8},{10,11... | collective-permute-start | bytes 1572872 | tf_op jit(solution)/shard_map/ppermute | solution.py:21
  142.4 12.8 %collective-permute-start.35 = (bf16[64,2048]{1,0:T(8,128)(2,1)S(1)}, bf16[64,2048]{1,0:T(8,128)(2,1)S(1)}, u32[]{:S(2)}, u32[]{:S(2)}) collective-permute-start(bf16[64,2048]{1,0:T(8,128)(2,1)S(1)} %add_convert_fusion.11), channel_id=1, source_target_pairs={{0,2},{1,3},{2,0},{3,1},{4,6},{5,7},{6,4},{7,5},{8,10},{9,11},{10,... | collective-permute-start | bytes 786440 | tf_op jit(solution)/shard_map/ppermute | solution.py:21
  150.4 15.0 %collective-permute-start.27 = (bf16[128,2048]{1,0:T(8,128)(2,1)S(1)}, bf16[128,2048]{1,0:T(8,128)(2,1)S(1)}, u32[]{:S(2)}, u32[]{:S(2)}) collective-permute-start(bf16[128,2048]{1,0:T(8,128)(2,1)S(1)} %add_convert_fusion.2), channel_id=1, source_target_pairs={{0,16},{4,20},{16,24},{20,28},{24,8},{28,12},{8,0},{12,4},{1,17},{... | collective-permute-start | bytes 1572872 | tf_op jit(solution)/shard_map/ppermute | solution.py:35
  165.9 13.3 %collective-permute-start.39 = (bf16[128,2048]{1,0:T(8,128)(2,1)S(1)}, bf16[128,2048]{1,0:T(8,128)(2,1)S(1)}, u32[]{:S(2)}, u32[]{:S(2)}) collective-permute-start(bf16[128,2048]{1,0:T(8,128)(2,1)S(1)} %add_convert_fusion.1), channel_id=1, source_target_pairs={{0,16},{4,20},{16,24},{20,28},{24,8},{28,12},{8,0},{12,4},{1,17},{... | collective-permute-start | bytes 1572872 | tf_op jit(solution)/shard_map/ppermute | solution.py:35
  166.0 11.8 %collective-permute-start.47 = (bf16[64,2048]{1,0:T(8,128)(2,1)S(1)}, bf16[64,2048]{1,0:T(8,128)(2,1)S(1)}, u32[]{:S(2)}, u32[]{:S(2)}) collective-permute-start(bf16[64,2048]{1,0:T(8,128)(2,1)S(1)} %add_convert_fusion.7), channel_id=1, source_target_pairs={{0,2},{1,3},{2,0},{3,1},{4,6},{5,7},{6,4},{7,5},{8,10},{9,11},{10,... | collective-permute-start | bytes 786440 | tf_op jit(solution)/shard_map/ppermute | solution.py:21
  (34 other events, 313.1 us)
